TPU v7x, 512 devices: a whole 4x8x8 slice. The times are simulated.
512 devices in a mesh: kv: 64 (over z, y), tp: 8 (over x, core).
Axes of the slice: x: 4, y: 8, z: 8, core: 2. Of those that a mesh axis runs over, the one named last changes fastest.
Arguments:
- queries: bfloat16 [8192, 1024], P('kv', 'tp'), may hold values from -4 to 4
- keys: bfloat16 [8192, 1024], P('kv', 'tp'), may hold values from -4 to 4
- values: bfloat16 [8192, 1024], P('kv', 'tp'), may hold values from -4 to 4
- cotangent: bfloat16 [8192, 1024], P('kv', 'tp'), may hold values from -4 to 4
- log_sum: float32 [16, 8192], P('tp', 'kv'), may hold values from 4.5 to 7.5
- chosen: int32 [16, 256, 12], P('tp'), may hold values from 0 to 255, as said below
- normed_input: bfloat16 [8192, 2048], P('kv', 'tp'), may hold values from -0.0625 to 0.0625
Outputs:
- grad_queries: bfloat16 [8192, 1024], P('kv', 'tp')
- grad_keys: bfloat16 [8192, 1024], P('kv', 'tp')
- grad_values: bfloat16 [8192, 1024], P('kv', 'tp')
- grad_weight: float32 [2048, 1024], P('kv', 'tp')
Inputs may be any that keep to these rules, and one draw needn't show every extreme that they name: `chosen`: for each head, the distinct blocks below their own query block that the query blocks of one device's 128 positions choose include at most 1 block of any one device's span of 128 positions, and exactly 1 for some pairs of devices. Within one list the entries below the query block's own index are distinct.
All inputs are finite; a program needn't handle non-finite values.
Results may differ from a plain program's by a relative error of at most 0.0085.
Values may be sent and summed in bfloat16 or wider, within the bound.
A program may use at most 64 MiB of HBM per device.

v0:
```python
import jax
import jax.numpy as jnp
from jax import lax
from jax.sharding import PartitionSpec as P

HD = 64
BLK = 32
SEL = 12
MOST = 1


MASKED = -1e30


def sent_together(arrays, axis, split_dim, concat_dim, along):
    both = jnp.concatenate(arrays, axis=along)
    whole, at, finished = (
        lax.all_to_all(both, axis, split_axis=split_dim, concat_axis=concat_dim, tiled=True),
        0,
        [],
    )
    for a in arrays:
        finished.append(lax.slice_in_dim(whole, at, at + a.shape[along], axis=along))
        at += a.shape[along]
    return tuple(finished)


def split_up(array, dim, size):
    dims = array.shape
    tiles = array.reshape(*dims[:dim], size, dims[dim] // size, *dims[dim + 1 :])
    return jnp.moveaxis(tiles, dim, 0)


def sum_at_owner(array, axis, dim):
    tiles = split_up(array, dim, lax.axis_size(axis))
    arrived = lax.all_to_all(tiles, axis, split_axis=0, concat_axis=0, tiled=True)
    return arrived.astype(jnp.float32).sum(axis=0)


def slot_picks(needed):
    span_width = needed.shape[-1]
    counted = needed.astype(jnp.int32)
    before = jnp.cumsum(counted, axis=-1) - counted
    places = jnp.arange(span_width, dtype=jnp.int32)
    picked, present = ([], [])
    hitting = needed & (before == 0)
    present.append(jnp.any(hitting, axis=-1))
    picked.append(jnp.sum(jnp.where(hitting, places, 0), axis=-1))
    return (jnp.stack(picked, axis=-1), jnp.stack(present, axis=-1))


def to_blocks(row_block, tok_rows, head_count):
    shards = row_block.shape[0] // tok_rows
    shaped = row_block.reshape(shards, tok_rows // BLK, BLK, head_count, HD).transpose(
        0, 3, 1, 2, 4
    )
    return shaped.reshape(shards * head_count * (tok_rows // BLK), BLK * HD)


def heads_from(row_block, head_count):
    blocks_dev = row_block.shape[0] // BLK
    return row_block.reshape(blocks_dev, BLK, head_count, HD).transpose(2, 0, 1, 3)


def back_rows(blocked):
    head_count, blocks_dev = (blocked.shape[0], blocked.shape[1])
    return blocked.transpose(1, 2, 0, 3).reshape(blocks_dev * BLK, head_count * HD)


def body(queries, keys, values, cotangent, log_sum, chosen, normed_input):
    tok_rows = queries.shape[0]
    head_count = log_sum.shape[0]
    blocks_dev = tok_rows // BLK
    devices = lax.axis_size("kv")
    my_index = lax.axis_index("kv")
    block_total = chosen.shape[1]
    tile_size = BLK * HD
    score_scale = HD ** (-0.5)
    places = jnp.arange(blocks_dev, dtype=jnp.int32)
    own_ids = my_index * blocks_dev + places
    my_lists = lax.dynamic_slice_in_dim(chosen, my_index * blocks_dev, blocks_dev, 1)
    usable = my_lists < own_ids[None, :, None]
    every_block = jnp.arange(block_total, dtype=jnp.int32)
    need_here = jnp.any((my_lists[..., None] == every_block) & usable[..., None], axis=(1, 2))
    req_picked, req_present = slot_picks(need_here.reshape(head_count, devices, blocks_dev))
    grouped = chosen.reshape(head_count, devices, blocks_dev, SEL)
    row_ids = every_block.reshape(devices, blocks_dev)
    usable_all = grouped < row_ids[None, :, :, None]
    need_there = jnp.any((grouped[..., None] == own_ids) & usable_all[..., None], axis=(2, 3))
    own_picked, own_present = slot_picks(need_there)
    own_picked = own_picked.transpose(1, 0, 2)
    own_present = own_present.transpose(1, 0, 2)
    head_base = (jnp.arange(head_count, dtype=jnp.int32) * blocks_dev)[None, :, None]
    send_ids = (head_base + own_picked).reshape(-1)
    key_send = jnp.take(to_blocks(keys, tok_rows, head_count), send_ids, axis=0).reshape(
        devices, head_count, MOST, tile_size
    )
    value_send = jnp.take(to_blocks(values, tok_rows, head_count), send_ids, axis=0).reshape(
        devices, head_count, MOST, tile_size
    )
    key_tiles, value_tiles = sent_together((key_send, value_send), "kv", 0, 0, 1)
    owners = my_lists // blocks_dev
    local_ids = my_lists % blocks_dev
    head_ids = jnp.arange(head_count, dtype=jnp.int32)[:, None, None]
    rows_at = (head_ids * devices + owners).reshape(-1)
    slot_at = jnp.take(req_picked.reshape(head_count * devices, MOST), rows_at, axis=0).reshape(
        head_count, blocks_dev, SEL, MOST
    )
    slot_live = jnp.take(req_present.reshape(head_count * devices, MOST), rows_at, axis=0).reshape(
        head_count, blocks_dev, SEL, MOST
    )
    matches = (slot_at == local_ids[..., None]) & slot_live
    slot_of = jnp.sum(jnp.where(matches, jnp.arange(MOST, dtype=jnp.int32), 0), axis=-1)
    tile_ids = jnp.where(usable, (owners * head_count + head_ids) * MOST + slot_of, 0).reshape(-1)
    sel_keys = jnp.take(key_tiles.reshape(-1, tile_size), tile_ids, axis=0).reshape(
        head_count, blocks_dev, SEL * BLK, HD
    )
    sel_values = jnp.take(value_tiles.reshape(-1, tile_size), tile_ids, axis=0).reshape(
        head_count, blocks_dev, SEL * BLK, HD
    )
    keys_all = jnp.concatenate([sel_keys, heads_from(keys, head_count)], axis=2)
    values_all = jnp.concatenate([sel_values, heads_from(values, head_count)], axis=2)
    causal = jnp.arange(BLK)[:, None] >= jnp.arange(BLK)[None, :]
    sel_mask = jnp.broadcast_to(
        jnp.repeat(usable, BLK, axis=2)[:, :, None, :], (head_count, blocks_dev, BLK, SEL * BLK)
    )
    allowed = jnp.concatenate(
        [sel_mask, jnp.broadcast_to(causal, (head_count, blocks_dev, BLK, BLK))], axis=3
    )
    q_blocks = heads_from(queries, head_count)
    g_blocks = heads_from(cotangent, head_count)
    log_rows = log_sum.reshape(head_count, blocks_dev, BLK)[..., None]
    scores = (
        jnp.einsum("hiqd,hikd->hiqk", q_blocks, keys_all, preferred_element_type=jnp.float32)
        * score_scale
    )
    weights = jnp.exp(jnp.where(allowed, scores - log_rows, MASKED))
    value_dots = jnp.einsum(
        "hiqd,hikd->hiqk", g_blocks, values_all, preferred_element_type=jnp.float32
    )
    row_delta = jnp.sum(weights * value_dots, axis=-1, keepdims=True)
    score_grad = (weights * (value_dots - row_delta)).astype(jnp.bfloat16)
    weights_low = weights.astype(jnp.bfloat16)
    query_grad = (
        jnp.einsum("hiqk,hikd->hiqd", score_grad, keys_all, preferred_element_type=jnp.float32)
        * score_scale
    )
    key_grad = (
        jnp.einsum("hiqk,hiqd->hikd", score_grad, q_blocks, preferred_element_type=jnp.float32)
        * score_scale
    )
    value_grad = jnp.einsum(
        "hiqk,hiqd->hikd", weights_low, g_blocks, preferred_element_type=jnp.float32
    )
    grad_queries = back_rows(query_grad).astype(jnp.bfloat16)

    def to_slots(gradient):
        chosen_part = gradient[:, :, : SEL * BLK].reshape(-1, tile_size)
        slotted = jax.ops.segment_sum(
            chosen_part, tile_ids, num_segments=devices * head_count * MOST
        )
        return slotted.reshape(devices, head_count, MOST, tile_size)

    back_keys, back_values = (
        lax.all_to_all(
            to_slots(key_grad).astype(jnp.bfloat16), "kv", split_axis=0, concat_axis=0, tiled=True
        ).astype(jnp.float32),
        lax.all_to_all(
            to_slots(value_grad).astype(jnp.bfloat16), "kv", split_axis=0, concat_axis=0, tiled=True
        ).astype(jnp.float32),
    )
    land_ids = jnp.where(own_present, head_base + own_picked, head_count * blocks_dev).reshape(-1)

    def settle(returned, gradient):
        flat_tiles = returned.reshape(-1, tile_size)
        targets = (
            jnp.arange(head_count * blocks_dev, dtype=jnp.int32)[:, None] == land_ids[None, :]
        ).astype(jnp.float32)
        landed = jnp.dot(
            targets, flat_tiles, precision=lax.Precision.HIGHEST, preferred_element_type=jnp.float32
        )
        summed = landed.reshape(head_count, blocks_dev, BLK, HD) + gradient[:, :, SEL * BLK :]
        return back_rows(summed).astype(jnp.bfloat16)

    grad_keys = settle(back_keys, key_grad)
    grad_values = settle(back_values, value_grad)
    whole_input = lax.all_gather(normed_input, "tp", axis=1, tiled=True)
    grad_weight = sum_at_owner(
        lax.dot_general(
            whole_input, grad_queries, (((0,), (0,)), ((), ())), preferred_element_type=jnp.float32
        ).astype(jnp.bfloat16),
        "kv",
        0,
    )
    return (grad_queries, grad_keys, grad_values, grad_weight)


def solution(mesh):
    in_specs = (
        P("kv", "tp"),
        P("kv", "tp"),
        P("kv", "tp"),
        P("kv", "tp"),
        P("tp", "kv"),
        P("tp", None, None),
        P("kv", "tp"),
    )
    out_specs = (P("kv", "tp"), P("kv", "tp"), P("kv", "tp"), P("kv", "tp"))
    return jax.shard_map(body, mesh=mesh, in_specs=in_specs, out_specs=out_specs, check_vma=False)
```

profile of v0, /device:TPU:6, one launch (start us, length us, event | category | flops | bytes accessed | tf_op | source)
XLA Modules:
  0.0 144.9 jit_solution(14934738471255190425)
XLA Ops:
  0.7 0.9 copy.75
  2.6 0.8 reshape.213
  3.9 0.9 gather_fusion
  4.8 0.9 gather_fusion.1
  6.6 2.1 %pad_maximum_fusion = bf16[64,4,1,2048]{3,1,2,0:T(4,128)(2,1)} fusion(bf16[64,2,1,2048]{3,1,2,0:T(2,128)(2,1)S(1)} %bitcast.101, bf16[64,2,1,2048]{3,1,2,0:T(2,128)(2,1)S(1)} %bitcast.102), kind=kLoop, calls=%fused_computation.18 | loop fusion | flops 2097152 | bytes 2097152 | tf_op jit(solution)/shard_map/concatenate | solution.py:16
  8.7 16.9 %all-to-all-start = ((bf16[64,4,1,2048]{3,1,2,0:T(4,128)(2,1)}), bf16[64,4,1,2048]{3,1,2,0:T(4,128)(2,1)S(1)}, u32[]{:S(2)}, u32[]{:S(2)}) async-start(bf16[64,4,1,2048]{3,1,2,0:T(4,128)(2,1)} %pad_maximum_fusion), calls=%async_computation | async-start | bytes 2097152 | tf_op jit(solution)/shard_map/all_to_all | solution.py:18
  27.1 28.1 %all-to-all-done = bf16[64,4,1,2048]{3,1,2,0:T(4,128)(2,1)S(1)} async-done(((bf16[64,4,1,2048]{3,1,2,0:T(4,128)(2,1)}), bf16[64,4,1,2048]{3,1,2,0:T(4,128)(2,1)S(1)}, u32[]{:S(2)}, u32[]{:S(2)}) %all-to-all-start) | async-done | bytes 1048608 | tf_op jit(solution)/shard_map/all_to_all | solution.py:18
  55.2 0.7 fusion.46
  56.4 0.8 gather_fusion.3
  57.2 0.8 gather_fusion.2
  58.2 0.8 reshape.226
  59.3 0.8 reshape.222
  63.1 2.0 %scatter_custom_fusion = f32[128,2048]{1,0:T(8,128)S(1)} fusion(s32[96]{0:T(128)S(1)} %reshape.221, f32[96,2048]{1,0:T(8,128)S(1)} %reshape.270, f32[]{:T(128)} %constant.105.clone.1), kind=kCustom, calls=%fused_computation.26 | custom fusion | flops 196608 | bytes 1048580 | tf_op jit(solution)/shard_map/scatter-add | solution.py:159
  65.2 1.2 convert_element_type.84
  66.4 6.7 %all-to-all-start.1 = ((bf16[64,2,1,2048]{3,1,2,0:T(2,128)(2,1)}), bf16[64,2,1,2048]{3,1,2,0:T(2,128)(2,1)}, u32[]{:S(2)}, u32[]{:S(2)}) async-start(bf16[64,2,1,2048]{3,1,2,0:T(2,128)(2,1)} %bitcast.18), calls=%async_computation.1 | async-start | bytes 1048576 | tf_op jit(solution)/shard_map/all_to_all | solution.py:165
  73.5 1.0 copy-done
  75.5 2.0 %scatter_custom_fusion.1 = f32[128,2048]{1,0:T(8,128)S(1)} fusion(s32[96]{0:T(128)S(1)} %reshape.221, f32[96,2048]{1,0:T(8,128)S(1)} %reshape.278, f32[]{:T(128)} %constant.105.clone.1), kind=kCustom, calls=%fused_computation.24 | custom fusion | flops 196608 | bytes 1048580 | tf_op jit(solution)/shard_map/scatter-add | solution.py:159
  77.6 1.1 convert_element_type.90
  78.8 13.0 %all-to-all-done.1 = bf16[64,2,1,2048]{3,1,2,0:T(2,128)(2,1)} async-done(((bf16[64,2,1,2048]{3,1,2,0:T(2,128)(2,1)}), bf16[64,2,1,2048]{3,1,2,0:T(2,128)(2,1)}, u32[]{:S(2)}, u32[]{:S(2)}) %all-to-all-start.1) | async-done | bytes 524320 | tf_op jit(solution)/shard_map/all_to_all | solution.py:165
  91.7 5.2 %all-to-all-start.2 = ((bf16[64,2,1,2048]{3,1,2,0:T(2,128)(2,1)}), bf16[64,2,1,2048]{3,1,2,0:T(2,128)(2,1)S(1)}, u32[]{:S(2)}, u32[]{:S(2)}) async-start(bf16[64,2,1,2048]{3,1,2,0:T(2,128)(2,1)} %bitcast.24), calls=%async_computation.2 | async-start | bytes 1048576 | tf_op jit(solution)/shard_map/all_to_all | solution.py:168
  97.2 13.1 %all_gather.3 = bf16[128,2048]{1,0:T(8,128)(2,1)S(1)} all-gather(bf16[128,256]{1,0:T(8,128)(2,1)S(1)} %copy-done.12), channel_id=1, replica_groups=mesh['kv'=64,'tp'=8] {'tp'}, dimensions={1}, use_global_device_ids=true | all-gather | bytes 589824 | tf_op jit(solution)/shard_map/all_gather | solution.py:187
  111.1 1.0 copy.101
  112.1 3.3 %all-to-all-done.2 = bf16[64,2,1,2048]{3,1,2,0:T(2,128)(2,1)S(1)} async-done(((bf16[64,2,1,2048]{3,1,2,0:T(2,128)(2,1)}), bf16[64,2,1,2048]{3,1,2,0:T(2,128)(2,1)S(1)}, u32[]{:S(2)}, u32[]{:S(2)}) %all-to-all-start.2) | async-done | bytes 524320 | tf_op jit(solution)/shard_map/all_to_all | solution.py:168
  115.4 9.4 %all-to-all-start.3 = ((bf16[64,32,128]{2,1,0:T(8,128)(2,1)}), bf16[64,32,128]{2,1,0:T(8,128)(2,1)S(1)}, u32[]{:S(2)}, u32[]{:S(2)}) async-start(bf16[64,32,128]{2,1,0:T(8,128)(2,1)} %bitcast.30), calls=%async_computation.3 | async-start | bytes 1048576 | tf_op jit(solution)/shard_map/all_to_all | solution.py:36
  124.8 1.2 reshape.230
  126.4 0.5 fusion.31
  127.2 0.7 convert_element_type.87
  128.4 0.5 fusion.29
  129.1 1.0 fusion.19
  130.2 0.7 convert_element_type.93
  130.9 13.3 %all-to-all-done.3 = bf16[64,32,128]{2,1,0:T(8,128)(2,1)S(1)} async-done(((bf16[64,32,128]{2,1,0:T(8,128)(2,1)}), bf16[64,32,128]{2,1,0:T(8,128)(2,1)S(1)}, u32[]{:S(2)}, u32[]{:S(2)}) %all-to-all-start.3) | async-done | bytes 524320 | tf_op jit(solution)/shard_map/all_to_all | solution.py:36
  144.2 0.7 convert_reduce_fusion
  (110 shorter events, 11.2 us)
Async XLA Ops:
  0.6 3.0 %copy-start.7 = (bf16[128,128]{1,0:T(8,128)(2,1)S(1)}, bf16[128,128]{1,0:T(8,128)(2,1)}, u32[]{:S(2)}) copy-start(bf16[128,128]{1,0:T(8,128)(2,1)} %param.13) | copy-start | bytes 98308
  8.7 17.0 %copy-start.8 = (bf16[128,128]{1,0:T(8,128)(2,1)S(1)}, bf16[128,128]{1,0:T(8,128)(2,1)}, u32[]{:S(2)}) copy-start(bf16[128,128]{1,0:T(8,128)(2,1)} %param.12) | copy-start | bytes 98308
  8.7 17.3 %copy-start.13 = (s32[2,256,12]{1,0,2:T(2,128)S(1)}, s32[2,256,12]{1,0,2:T(2,128)}, u32[]{:S(2)}) copy-start(s32[2,256,12]{1,0,2:T(2,128)} %param.16) | copy-start | bytes 73732
  8.7 17.6 %copy-start.14 = (bf16[128,128]{1,0:T(8,128)(2,1)S(1)}, bf16[128,128]{1,0:T(8,128)(2,1)}, u32[]{:S(2)}) copy-start(bf16[128,128]{1,0:T(8,128)(2,1)} %param.14) | copy-start | bytes 98308
  8.7 17.7 %copy-start.16 = (f32[2,128]{1,0:T(2,128)S(1)}, f32[2,128]{1,0:T(2,128)}, u32[]{:S(2)}) copy-start(f32[2,128]{1,0:T(2,128)} %param.15) | copy-start | bytes 3076
  8.7 17.9 %copy-start.15 = (bf16[128,128]{1,0:T(8,128)(2,1)S(1)}, bf16[128,128]{1,0:T(8,128)(2,1)}, u32[]{:S(2)}) copy-start(bf16[128,128]{1,0:T(8,128)(2,1)} %param.11) | copy-start | bytes 98308
  8.7 46.5 %all-to-all-start = ((bf16[64,4,1,2048]{3,1,2,0:T(4,128)(2,1)}), bf16[64,4,1,2048]{3,1,2,0:T(4,128)(2,1)S(1)}, u32[]{:S(2)}, u32[]{:S(2)}) async-start(bf16[64,4,1,2048]{3,1,2,0:T(4,128)(2,1)} %pad_maximum_fusion), calls=%async_computation | async-start | bytes 2097152 | tf_op jit(solution)/shard_map/all_to_all | solution.py:18
  26.6 34.1 %copy-start.10 = (bf16[4,32,2,64]{1,3,0,2:T(8,128)(2,1)}, bf16[4,32,2,64]{1,3,0,2:T(8,128)(2,1)S(1)}, u32[]{:S(2)}) copy-start(bf16[4,32,2,64]{1,3,0,2:T(8,128)(2,1)S(1)} %copy.83) | copy-start | bytes 98308
  60.4 0.8 copy-start.5
  61.2 0.8 copy-start.1
  61.3 0.8 copy-start.3
  65.1 8.0 %copy-start.2 = (f32[2,4,32,416]{3,2,1,0:T(8,128)S(1)}, f32[2,4,32,416]{3,2,1,0:T(8,128)}, u32[]{:S(2)}) copy-start(f32[2,4,32,416]{3,2,1,0:T(8,128)} %copy-done.1) | copy-start | bytes 1277956
  66.4 25.4 %all-to-all-start.1 = ((bf16[64,2,1,2048]{3,1,2,0:T(2,128)(2,1)}), bf16[64,2,1,2048]{3,1,2,0:T(2,128)(2,1)}, u32[]{:S(2)}, u32[]{:S(2)}) async-start(bf16[64,2,1,2048]{3,1,2,0:T(2,128)(2,1)} %bitcast.18), calls=%async_computation.1 | async-start | bytes 1048576 | tf_op jit(solution)/shard_map/all_to_all | solution.py:165
  73.5 1.0 copy-start
  77.5 19.6 %copy-start.12 = (bf16[128,256]{1,0:T(8,128)(2,1)S(1)}, bf16[128,256]{1,0:T(8,128)(2,1)}, u32[]{:S(2)}) copy-start(bf16[128,256]{1,0:T(8,128)(2,1)} %param.17) | copy-start | bytes 196612
  77.6 32.7 %copy-start.4 = (bf16[2,4,32,416]{3,2,1,0:T(8,128)(2,1)S(1)}, bf16[2,4,32,416]{3,2,1,0:T(8,128)(2,1)}, u32[]{:S(2)}) copy-start(bf16[2,4,32,416]{3,2,1,0:T(8,128)(2,1)} %copy-done.3) | copy-start | bytes 638980
  77.6 32.7 %copy-start.6 = (bf16[2,4,384,64]{2,3,1,0:T(8,128)(2,1)S(1)}, bf16[2,4,384,64]{2,3,1,0:T(8,128)(2,1)}, u32[]{:S(2)}) copy-start(bf16[2,4,384,64]{2,3,1,0:T(8,128)(2,1)} %copy-done.5) | copy-start | bytes 1179652
  77.6 32.7 %copy-start.11 = (bf16[4,32,2,64]{1,3,0,2:T(8,128)(2,1)S(1)}, bf16[4,32,2,64]{1,3,0,2:T(8,128)(2,1)}, u32[]{:S(2)}) copy-start(bf16[4,32,2,64]{1,3,0,2:T(8,128)(2,1)} %copy-done.10) | copy-start | bytes 98308
  91.7 23.6 %all-to-all-start.2 = ((bf16[64,2,1,2048]{3,1,2,0:T(2,128)(2,1)}), bf16[64,2,1,2048]{3,1,2,0:T(2,128)(2,1)S(1)}, u32[]{:S(2)}, u32[]{:S(2)}) async-start(bf16[64,2,1,2048]{3,1,2,0:T(2,128)(2,1)} %bitcast.24), calls=%async_computation.2 | async-start | bytes 1048576 | tf_op jit(solution)/shard_map/all_to_all | solution.py:168
  110.7 4.6 %copy-start.9 = (bf16[128,128]{1,0:T(8,128)(2,1)}, bf16[128,128]{1,0:T(8,128)(2,1)S(1)}, u32[]{:S(2)}) copy-start(bf16[128,128]{1,0:T(8,128)(2,1)S(1)} %convert_element_type.82) | copy-start | bytes 98308
  115.4 28.8 %all-to-all-start.3 = ((bf16[64,32,128]{2,1,0:T(8,128)(2,1)}), bf16[64,32,128]{2,1,0:T(8,128)(2,1)S(1)}, u32[]{:S(2)}, u32[]{:S(2)}) async-start(bf16[64,32,128]{2,1,0:T(8,128)(2,1)} %bitcast.30), calls=%async_computation.3 | async-start | bytes 1048576 | tf_op jit(solution)/shard_map/all_to_all | solution.py:36
where the time goes:
time: 146 us; the launch traced here: 145 us
  waiting for transfers between devices  57.7 us (40%)
  starting transfers between devices  38.3 us (26%)
  local copies, waits for them, and re-layouts  22.7 us (16%)
  blocking collectives  13.1 us (9%)
  other arithmetic  8.99 us (6%)
  matrix products  2.89 us (2%)
    all_to_all x1, waiting for transfers between devices, sent_together(): lax.all_to_all(both, axis, split_axis=split_dim, concat_axis=concat_dim,...  28.1 us
    all_to_all x1, starting transfers between devices, sent_together(): lax.all_to_all(both, axis, split_axis=split_dim, concat_axis=concat_dim,...  16.9 us
    all_to_all x1, waiting for transfers between devices, sum_at_owner(): lax.all_to_all(tiles, axis, split_axis=0, concat_axis=0, tiled=True)  13.3 us
    all_gather x1, blocking collectives, body(): whole_input = lax.all_gather(normed_input, 'tp', axis=1, tiled=True)  13.1 us
    all_to_all x1, waiting for transfers between devices, body(): lax.all_to_all(to_slots(key_grad).astype(jnp.bfloat16), 'kv', split_axis=...  13 us
    all_to_all x1, starting transfers between devices, sum_at_owner(): lax.all_to_all(tiles, axis, split_axis=0, concat_axis=0, tiled=True)  9.43 us
    all_to_all x1, starting transfers between devices, body(): lax.all_to_all(to_slots(key_grad).astype(jnp.bfloat16), 'kv', split_axis=...  6.75 us
    all_to_all x1, starting transfers between devices, body(): lax.all_to_all(to_slots(value_grad).astype(jnp.bfloat16), 'kv', split_axi...  5.19 us
  transfers between devices with their start and end apart: 4, of which 4 were waited for; matrix products, arithmetic and copies ran while one was open for 10% of the time, Pallas kernels for 0%

commit v1 on v0

v1 whole, which is shorter than its diff:
```python
import jax
import jax.numpy as jnp
from jax import lax
from jax.experimental import pallas as pl
from jax.experimental.pallas import tpu as pltpu
from jax.sharding import PartitionSpec as P

HD = 64
BLK = 32
SEL = 12
MASKED = -1e30
RING = 8
TOK = 128
COLS = 128
OFFS = (0, 1, 7, 2, 6, 3, 5, 4)
MESH = pl.DeviceIdType.MESH
F32 = jnp.float32
BF16 = jnp.bfloat16


def nt(a, b):
    return lax.dot_general(a, b, (((1,), (1,)), ((), ())), preferred_element_type=F32)


def nn(a, b):
    return lax.dot_general(a, b, (((1,), (0,)), ((), ())), preferred_element_type=F32)


def kernel(
    q_in, k_in, v_in, g_in, ls_in, ch_in, x_in,
    dq_out, dk_out, dv_out, gw_out,
    qg, kv, ls, xg, chs, qm, gm, kt, xt, bias, wf, dpf, w16, ds16, dl,
    dvs, dvr, dks, dkr, dqs, dqr, gas, gar, gbs, gbr, ha_s, ha_r, hb_s, hb_r,
    loc, sq, rq, sl, rl, sk, rk, sx, rx, sd, rd, sv, rv, sdk, rdk, sdq, rdq,
    sga, rga, sgb, rgb, sha, rha, shb, rhb,
):
    me = lax.axis_index("kv")
    tp = lax.axis_index("tp")
    z = me // RING
    y = me % RING

    def ring(base, off):
        return (base + off) % RING

    def along_y(off):
        return (z * RING + ring(y, off), tp)

    def along_z(off):
        return (ring(z, off) * RING + y, tp)

    def along_tp(off):
        return (me, ring(tp, off))

    def remote(src, dst, send, recv, target):
        return pltpu.make_async_remote_copy(
            src_ref=src, dst_ref=dst, send_sem=send, recv_sem=recv, device_id=target, device_id_type=MESH
        )

    barrier = pltpu.get_barrier_semaphore()
    for off in range(1, RING):
        for target in (along_y(off), along_z(off), along_tp(off)):
            pl.semaphore_signal(barrier, inc=1, device_id=target, device_id_type=MESH)

    first, second = pl.ds(0, TOK), pl.ds(TOK, TOK)
    locals_ = [
        pltpu.make_async_copy(q_in, qg.at[y, first], loc.at[0]),
        pltpu.make_async_copy(g_in, qg.at[y, second], loc.at[1]),
        pltpu.make_async_copy(k_in, kv.at[z, first], loc.at[2]),
        pltpu.make_async_copy(v_in, kv.at[z, second], loc.at[3]),
        pltpu.make_async_copy(ls_in, ls.at[y], loc.at[4]),
        pltpu.make_async_copy(x_in, xg.at[tp], loc.at[5]),
        pltpu.make_async_copy(ch_in.at[:, pl.ds(z * 32, 32)], chs, loc.at[6]),
    ]
    for c in locals_:
        c.start()
    for c in locals_:
        c.wait()
    pl.semaphore_wait(barrier, 3 * (RING - 1))

    pending = []

    def send(src, dst, ssem, rsem, target):
        c = remote(src, dst, ssem, rsem, target)
        c.start()
        pending.append(c)

    for i, off in enumerate(OFFS[1:]):
        send(qg.at[y], qg.at[y], sq.at[i], rq.at[y], along_y(off))
        send(ls.at[y], ls.at[y], sl.at[i], rl.at[y], along_y(off))
        send(kv.at[z], kv.at[z], sk.at[i], rk.at[z], along_z(off))
    for i, off in enumerate(OFFS[1:]):
        send(xg.at[tp], xg.at[tp], sx.at[i], rx.at[tp], along_tp(off))

    spread = (
        lax.broadcasted_iota(jnp.int32, (32, 1024), 1) // BLK
        == lax.broadcasted_iota(jnp.int32, (32, 1024), 0)
    ).astype(BF16)
    own_id = (lax.broadcasted_iota(jnp.int32, (1, 1024), 1) // BLK + z * 32).astype(F32)
    for h in range(2):
        lists = lax.dot_general(
            chs[h].astype(F32).astype(BF16), spread, (((0,), (0,)), ((), ())), preferred_element_type=F32
        )

        def one_column(zz, _, h=h, lists=lists):
            block = ((zz * RING + y) * 4 + lax.broadcasted_iota(jnp.int32, (4, 1024), 0)).astype(F32)
            hit = jnp.zeros((4, 1024), F32)
            for s in range(SEL):
                hit = jnp.where(block == lists[s : s + 1, :], 1.0, hit)
            hit = jnp.where(block < own_id, hit, 0.0)
            hit = jnp.where(block == own_id, 1.0, hit)
            bias[h, zz] = jnp.where(hit > 0.5, 0.0, MASKED)
            return 0

        lax.fori_loop(0, RING, one_column, 0)

    head0 = lax.broadcasted_iota(jnp.int32, (TOK, COLS), 1) < HD
    zero = jnp.zeros((TOK, COLS), BF16)

    def stage_q(yy):
        for src, dst in ((first, qm), (second, gm)):
            tile = qg[yy, src, :]
            dst[yy, first, :] = jnp.where(head0, tile, zero)
            dst[yy, second, :] = jnp.where(head0, zero, tile)

    def stage_k(zz):
        tile = kv[zz, first, :]
        kt[:, pl.ds(pl.multiple_of(zz * TOK, TOK), TOK)] = tile.astype(F32).T.astype(BF16)

    for off in OFFS:
        if off:
            yy, zz = ring(y, off), ring(z, off)
            remote(qg.at[yy], qg.at[yy], sq.at[0], rq.at[yy], along_y(off)).wait_recv()
            remote(ls.at[yy], ls.at[yy], sl.at[0], rl.at[yy], along_y(off)).wait_recv()
            remote(kv.at[zz], kv.at[zz], sk.at[0], rk.at[zz], along_z(off)).wait_recv()

    def stage(i, _):
        stage_q(i)
        stage_k(i)
        return 0

    lax.fori_loop(0, RING, stage, 0)

    row_i = lax.broadcasted_iota(jnp.int32, (TOK, TOK), 0)
    col_i = lax.broadcasted_iota(jnp.int32, (TOK, TOK), 1)
    future = (row_i // BLK == col_i // BLK) & (row_i > col_i)
    diag_bias = jnp.where(future, MASKED, 0.0).astype(F32)
    dl[y] = jnp.zeros((16, TOK), F32)

    def strip(zz, _):
        k_tile = kv[zz, first, :]
        v_tile = kv[zz, second, :]
        for yy in range(RING):
            s = nt(k_tile, qm[yy])
            dp = nt(v_tile, gm[yy])
            own = jnp.where((zz == z) & (yy == y), 1.0, 0.0).astype(F32)
            for h in range(2):
                lanes = slice(h * TOK, (h + 1) * TOK)
                rows = bias[h, zz, :, yy * TOK : (yy + 1) * TOK] - ls[yy, h : h + 1, :]
                rows = jnp.concatenate(
                    [jnp.broadcast_to(rows[b : b + 1], (BLK, TOK)) for b in range(4)], axis=0
                )
                w = jnp.exp(s[:, lanes] * 0.125 + rows + own * diag_bias)
                d = dp[:, lanes]
                at = yy * 256 + h * TOK
                wf[zz, :, at : at + TOK] = w
                dpf[zz, :, at : at + TOK] = d
                w16[zz, :, at : at + TOK] = w.astype(BF16)
                r = yy * 2 + h
                dl[y, r : r + 1, :] += jnp.sum(w * d, axis=0, keepdims=True)
        return 0

    lax.fori_loop(0, RING, strip, 0)

    for i, off in enumerate(OFFS[1:]):
        send(dl.at[y], dl.at[y], sd.at[i], rd.at[y], along_y(off))

    def value_grad(zz, _):
        dvs[zz] = nn(w16[zz], gm[...].reshape(2048, COLS)).astype(BF16)
        return 0

    lax.fori_loop(0, RING, value_grad, 0)
    for i, off in enumerate(OFFS[1:]):
        send(dvs.at[ring(z, off)], dvr.at[z], sv.at[i], rv.at[z], along_z(off))

    for off in range(1, RING):
        t = ring(tp, off)
        remote(xg.at[t], xg.at[t], sx.at[0], rx.at[t], along_tp(off)).wait_recv()

    def turn(t, _):
        xt[pl.ds(pl.multiple_of(t * 256, 256), 256), :] = xg[t].astype(F32).T.astype(BF16)
        return 0

    lax.fori_loop(0, RING, turn, 0)

    total = dl[y]
    for off in range(1, RING):
        yy = ring(y, off)
        remote(dl.at[yy], dl.at[yy], sd.at[0], rd.at[yy], along_y(off)).wait_recv()
        total = total + dl[yy]

    for yy in range(RING):
        for h in range(2):
            at = yy * 256 + h * TOK
            drow = total[yy * 2 + h : yy * 2 + h + 1, :]

            def score_grad(zz, _, at=at, drow=drow):
                ds16[zz, :, at : at + TOK] = (
                    wf[zz, :, at : at + TOK] * (dpf[zz, :, at : at + TOK] - drow)
                ).astype(BF16)
                return 0

            lax.fori_loop(0, RING, score_grad, 0)

    def query_grad(yy, _):
        lanes0 = pl.ds(pl.multiple_of(yy * 256, 256), 256)
        both = nn(kt[...], ds16[:, :, lanes0].reshape(1024, 256))
        dqs[yy, 0:HD, :] = both[0:HD, 0:TOK].astype(BF16)
        dqs[yy, HD:COLS, :] = both[HD:COLS, TOK:256].astype(BF16)
        return 0

    lax.fori_loop(0, RING, query_grad, 0)
    for i, off in enumerate(OFFS[1:]):
        send(dqs.at[ring(y, off)], dqr.at[y], sdq.at[i], rdq.at[y], along_y(off))

    def key_grad(zz, _):
        dks[zz] = nn(ds16[zz], qm[...].reshape(2048, COLS)).astype(BF16)
        return 0

    lax.fori_loop(0, RING, key_grad, 0)
    for i, off in enumerate(OFFS[1:]):
        send(dks.at[ring(z, off)], dkr.at[z], sdk.at[i], rdk.at[z], along_z(off))

    acc = dqs[y].astype(F32)
    for off in OFFS[1:]:
        yy = ring(y, off)
        remote(dqs.at[yy], dqr.at[yy], sdq.at[0], rdq.at[yy], along_y(off)).wait_recv()
        acc = acc + dqr[yy].astype(F32)
    dq = (acc * 0.125).T.astype(BF16)
    dq_out[...] = dq

    def weight_part(zz, _):
        part = nn(xt[pl.ds(pl.multiple_of(zz * 256, 256), 256), :], dq)
        part = part.astype(BF16).reshape(RING, 2, 16, COLS)
        gas[zz] = part[:, 0]
        gbs[:, zz] = part[:, 1]
        return 0

    lax.fori_loop(0, RING, weight_part, 0)
    for i, off in enumerate(OFFS[1:]):
        send(gas.at[ring(z, off)], gar.at[z], sga.at[i], rga.at[z], along_z(off))
        send(gbs.at[ring(y, off)], gbr.at[y], sgb.at[i], rgb.at[y], along_y(off))

    acc = dvs[z].astype(F32)
    for off in OFFS[1:]:
        zz = ring(z, off)
        remote(dvs.at[zz], dvr.at[zz], sv.at[0], rv.at[zz], along_z(off)).wait_recv()
        acc = acc + dvr[zz].astype(F32)
    dv_out[...] = acc.astype(BF16)

    acc = dks[z].astype(F32)
    for off in OFFS[1:]:
        zz = ring(z, off)
        remote(dks.at[zz], dkr.at[zz], sdk.at[0], rdk.at[zz], along_z(off)).wait_recv()
        acc = acc + dkr[zz].astype(F32)
    dk_out[...] = (acc * 0.125).astype(BF16)

    acc = gas[z].astype(F32)
    for off in OFFS[1:]:
        zz = ring(z, off)
        remote(gas.at[zz], gar.at[zz], sga.at[0], rga.at[zz], along_z(off)).wait_recv()
        acc = acc + gar[zz].astype(F32)
    ha_s[...] = acc.astype(BF16)
    for i, off in enumerate(OFFS[1:]):
        send(ha_s.at[ring(y, off)], ha_r.at[y], sha.at[i], rha.at[y], along_y(off))

    acc = gbs[y].astype(F32)
    for off in OFFS[1:]:
        yy = ring(y, off)
        remote(gbs.at[yy], gbr.at[yy], sgb.at[0], rgb.at[yy], along_y(off)).wait_recv()
        acc = acc + gbr[yy].astype(F32)
    hb_s[...] = acc.astype(BF16)
    for i, off in enumerate(OFFS[1:]):
        send(hb_s.at[ring(z, off)], hb_r.at[z], shb.at[i], rhb.at[z], along_z(off))

    acc = ha_s[y].astype(F32)
    for off in OFFS[1:]:
        yy = ring(y, off)
        remote(ha_s.at[yy], ha_r.at[yy], sha.at[0], rha.at[yy], along_y(off)).wait_recv()
        acc = acc + ha_r[yy].astype(F32)
    gw_out[0:16, :] = acc

    acc = hb_s[z].astype(F32)
    for off in OFFS[1:]:
        zz = ring(z, off)
        remote(hb_s.at[zz], hb_r.at[zz], shb.at[0], rhb.at[zz], along_z(off)).wait_recv()
        acc = acc + hb_r[zz].astype(F32)
    gw_out[16:32, :] = acc

    for c in pending:
        c.wait_send()


def body(queries, keys, values, cotangent, log_sum, chosen, normed_input):
    vm = pltpu.VMEM
    dma = pltpu.SemaphoreType.DMA
    scratch = [
        vm((8, 256, 128), BF16),
        vm((8, 256, 128), BF16),
        vm((8, 2, 128), F32),
        vm((8, 128, 256), BF16),
        vm((2, 32, SEL), jnp.int32),
        vm((8, 256, 128), BF16),
        vm((8, 256, 128), BF16),
        vm((128, 1024), BF16),
        vm((2048, 128), BF16),
        vm((2, 8, 4, 1024), F32),
        vm((8, 128, 2048), F32),
        vm((8, 128, 2048), F32),
        vm((8, 128, 2048), BF16),
        vm((8, 128, 2048), BF16),
        vm((8, 16, 128), F32),
    ]
    scratch += [vm((8, 128, 128), BF16)] * 6
    scratch += [vm((8, 8, 16, 128), BF16)] * 4
    scratch += [vm((8, 16, 128), BF16)] * 4
    scratch += [dma((7,))]
    scratch += [dma((8,))] * 24
    return pl.pallas_call(
        kernel,
        out_shape=(
            jax.ShapeDtypeStruct((TOK, COLS), BF16),
            jax.ShapeDtypeStruct((TOK, COLS), BF16),
            jax.ShapeDtypeStruct((TOK, COLS), BF16),
            jax.ShapeDtypeStruct((32, COLS), F32),
        ),
        in_specs=[pl.BlockSpec(memory_space=pl.ANY)] * 7,
        out_specs=[pl.BlockSpec(memory_space=pltpu.VMEM)] * 4,
        scratch_shapes=scratch,
        compiler_params=pltpu.CompilerParams(
            collective_id=0, has_side_effects=True, vmem_limit_bytes=60 * 1024 * 1024
        ),
    )(queries, keys, values, cotangent, log_sum, chosen, normed_input)


def solution(mesh):
    in_specs = (
        P("kv", "tp"),
        P("kv", "tp"),
        P("kv", "tp"),
        P("kv", "tp"),
        P("tp", "kv"),
        P("tp", None, None),
        P("kv", "tp"),
    )
    out_specs = (P("kv", "tp"), P("kv", "tp"), P("kv", "tp"), P("kv", "tp"))
    return jax.shard_map(body, mesh=mesh, in_specs=in_specs, out_specs=out_specs, check_vma=False)
```

time: 146 us -> 73.6 us (0.50)
  Pallas kernels: 0 us -> 67.2 us
  waiting for transfers between devices: 57.7 us -> 0 us
  starting transfers between devices: 38.3 us -> 0 us
  local copies, waits for them, and re-layouts: 22.7 us -> 5.06 us
  blocking collectives: 13.1 us -> 0 us
  other arithmetic: 8.99 us -> 0 us
  matrix products: 2.89 us -> 0 us
    pallas_call x0 -> x1, Pallas kernels: none -> 67.2 us  [body(): pl.pallas_call(kernel, out_shape=(jax.ShapeDtypeStruct((TOK, COLS), BF16)...]
    all_to_all x4 -> x0, waiting for transfers between devices: 57.7 us -> none  [the longest x1 28.1 us: sent_together(): lax.all_to_all(both, axis, split_axis=split_dim, concat_axis=concat_dim,...]
    all_to_all x4 -> x0, starting transfers between devices: 38.3 us -> none  [the longest x1 16.9 us: sent_together(): lax.all_to_all(both, axis, split_axis=split_dim, concat_axis=concat_dim,...]
    all_gather x1 -> x0, blocking collectives: 13.1 us -> none  [body(): whole_input = lax.all_gather(normed_input, 'tp', axis=1, tiled=True)]
    reshape x26 -> x0, local copies, waits for them, and re-layouts: 7.78 us -> none  [the longest x2 1.44 us: settle(): flat_tiles = returned.reshape(-1, tile_size)]
    convert_element_type x9 -> x0, local copies, waits for them, and re-layouts: 5.13 us -> none  [the longest x4 1.65 us: settle(): return back_rows(summed).astype(jnp.bfloat16)]
    scatter-add x2 -> x0, other arithmetic: 4.01 us -> none  [to_slots(): jax.ops.segment_sum(chosen_part, tile_ids, num_segments=devices * head_co...]
    gather x4 -> x0, local copies, waits for them, and re-layouts: 3.54 us -> none  [the longest x1 0.94 us: body(): jnp.take(to_blocks(values, tok_rows, head_count), send_ids, axis=0)]
  transfers between devices with their start and end apart: 4 -> 0, of which waited for: 4 -> 0; matrix products, arithmetic and copies ran while one was open for 10% -> 0% of each run, Pallas kernels for 0% -> 0%
where the time goes in v1:
time: 73.6 us; the launch traced here: 72.9 us
  Pallas kernels  67.2 us (91%)
  local copies, waits for them, and re-layouts  5.06 us (7%)
    pallas_call x1, Pallas kernels, body(): pl.pallas_call(kernel, out_shape=(jax.ShapeDtypeStruct((TOK, COLS), BF16)...  67.2 us
    unnamed x11, local copies, waits for them, and re-layouts  5.06 us

profile of v1, /device:TPU:6, one launch (start us, length us, event | category | flops | bytes accessed | tf_op | source)
XLA Modules:
  0.0 72.9 jit_solution(6822596856848593005)
XLA Ops:
  0.6 1.6 %copy.11.ch_in = s32[2,256,12]{2,1,0:T(8,128)} copy(s32[2,256,12]{1,0,2:T(2,128)} %param.12) | data formatting | bytes 49152 | tf_op args[5]
  2.2 67.2 %shard_map.102 = (bf16[128,128]{1,0:T(8,128)(2,1)}, bf16[128,128]{1,0:T(8,128)(2,1)}, bf16[128,128]{1,0:T(8,128)(2,1)}, f32[32,128]{1,0:T(8,128)}) custom-call(bf16[128,128]{1,0:T(8,128)(2,1)} %q_in.1, bf16[128,128]{1,0:T(8,128)(2,1)} %k_in.1, bf16[128,128]{1,0:T(8,128)(2,1)} %v_in.1, bf16[128,128]{1,0:T(8,128)(2,1)} %g_in.1, f32[2,128]{1,0:T(2,128)} %ls_in.1, ...), custom_call_target="tpu_custom_call" | custom-call | tf_op jit(solution)/shard_map/pallas_call | solution.py:328
  69.4 0.0 copy-start.1
  69.4 1.4 %copy.16 = bf16[128,128]{1,0:T(8,128)(2,1)} copy(bf16[128,128]{1,0:T(8,128)(2,1)} %get-tuple-element.8) | data formatting | bytes 65536
  70.8 0.0 copy-done.1
  70.8 0.0 copy-start
  70.8 0.6 copy.17
  71.4 0.2 copy-done
  71.5 0.0 copy-start.2
  71.5 0.6 copy.18
  72.2 0.1 copy-done.2
  72.3 0.6 copy.19
Async XLA Ops:
  69.4 1.4 %copy-start.1 = (bf16[128,128]{1,0:T(8,128)(2,1)S(1)}, bf16[128,128]{1,0:T(8,128)(2,1)}, u32[]{:S(2)}) copy-start(bf16[128,128]{1,0:T(8,128)(2,1)} %get-tuple-element.9) | copy-start | bytes 98308
  70.8 0.8 %copy-start = (bf16[128,128]{1,0:T(8,128)(2,1)S(1)}, bf16[128,128]{1,0:T(8,128)(2,1)}, u32[]{:S(2)}) copy-start(bf16[128,128]{1,0:T(8,128)(2,1)} %get-tuple-element.10) | copy-start | bytes 98308
  71.5 0.7 %copy-start.2 = (f32[32,128]{1,0:T(8,128)S(1)}, f32[32,128]{1,0:T(8,128)}, u32[]{:S(2)}) copy-start(f32[32,128]{1,0:T(8,128)} %get-tuple-element.11) | copy-start | bytes 49156

commit v2 on v1

v2 whole, which is shorter than its diff:
```python
import jax
import jax.numpy as jnp
from jax import lax
from jax.experimental import pallas as pl
from jax.experimental.pallas import tpu as pltpu
from jax.sharding import PartitionSpec as P

HD = 64
BLK = 32
SEL = 12
MASKED = -1e30
RING = 8
TOK = 128
COLS = 128
ORDER = (0, 2, -2, 1, -1, 3, -3, 4)
POS = {off % RING: i for i, off in enumerate(ORDER)}
FAR = (4, 3, -3, 2, -2, 1, -1)
MESH = pl.DeviceIdType.MESH
F32 = jnp.float32
BF16 = jnp.bfloat16


def nt(a, b):
    return lax.dot_general(a, b, (((1,), (1,)), ((), ())), preferred_element_type=F32)


def nn(a, b):
    return lax.dot_general(a, b, (((1,), (0,)), ((), ())), preferred_element_type=F32)


def kernel(
    q_in, k_in, v_in, g_in, ls_in, ch_in, x_in,
    dq_out, dk_out, dv_out, gw_out,
    qg, kv, ls, xg, chs, qm, gm, kt, xt, bias, wf, dpf, w16, ds16, da, dl,
    dvs, dvr, dks, dkr, dqs, dqr, gas, gar, gbs, gbr, ha_s, ha_r, hb_s, hb_r,
    loc, gq, gk, done, come,
):
    me = lax.axis_index("kv")
    tp = lax.axis_index("tp")
    z = me // RING
    y = me % RING

    def ring(base, off):
        return (base + off + RING) % RING

    def along_y(off):
        return (z * RING + ring(y, off), tp)

    def along_z(off):
        return (ring(z, off) * RING + y, tp)

    def along_tp(off):
        return (me, ring(tp, off))

    def remote(src, dst, send, recv, target):
        return pltpu.make_async_remote_copy(
            src_ref=src, dst_ref=dst, send_sem=send, recv_sem=recv, device_id=target, device_id_type=MESH
        )

    def slot(off):
        return POS[off % RING]

    barrier = pltpu.get_barrier_semaphore()
    for off in range(1, RING):
        for target in (along_y(off), along_z(off), along_tp(off)):
            pl.semaphore_signal(barrier, inc=1, device_id=target, device_id_type=MESH)

    first, second = pl.ds(0, TOK), pl.ds(TOK, TOK)
    loads = [
        pltpu.make_async_copy(q_in, qg.at[0, first], loc.at[0]),
        pltpu.make_async_copy(k_in, kv.at[0, first], loc.at[1]),
        pltpu.make_async_copy(g_in, qg.at[0, second], loc.at[2]),
        pltpu.make_async_copy(v_in, kv.at[0, second], loc.at[3]),
        pltpu.make_async_copy(ls_in, ls.at[0], loc.at[4]),
        pltpu.make_async_copy(x_in, xg.at[0], loc.at[5]),
        pltpu.make_async_copy(ch_in, chs, loc.at[6]),
    ]
    for c in loads:
        c.start()
    for c in loads:
        c.wait()
    pl.semaphore_wait(barrier, 3 * (RING - 1))

    halves = (first, second)
    rings = ((qg, along_y, gq, 0), (kv, along_z, gk, 1))
    steps = [(half, r, d) for half in (0, 1) for r in rings for d in (1, -1)]

    def group(off, half):
        near = (off + 4) % RING - 4
        if abs(near) == 2:
            return (0 if near < 0 else 2) + half
        return {1: 4, 3: 5, 4: 6}[abs(near)]

    def pass_on(r, src, half, hop):
        buf, along, sems, n = r
        where = buf.at[slot(src), halves[half]]
        remote(
            where, buf.at[slot(src - hop), halves[half]], done.at[n], sems.at[group(src - hop, half)], along(hop)
        ).start()

    for half, r, d in steps:
        pass_on(r, 0, half, 2 * d)
    for r in rings:
        for d in (1, -1):
            buf, along, sems, n = r
            remote(buf.at[0], buf.at[slot(-d)], done.at[n], sems.at[4], along(d)).start()
    for off in FAR:
        remote(ls.at[0], ls.at[slot(-off)], done.at[2], come.at[2], along_y(off)).start()
    for off in range(1, RING):
        remote(xg.at[0], xg.at[RING - off], done.at[3], come.at[3], along_tp(off)).start()

    lane = lax.broadcasted_iota(jnp.int32, (1, TOK), 1) // BLK
    own_id = jnp.concatenate([(z * RING + ring(y, off)) * 4 + lane for off in ORDER], axis=1)
    spread = (lax.broadcasted_iota(jnp.int32, (256, 1024), 0) == own_id).astype(BF16)
    own_id = own_id.astype(F32)
    lists = [nn(chs[:, h, :].astype(F32).astype(BF16), spread) for h in range(2)]
    for i, off in enumerate(ORDER):
        block = (lax.broadcasted_iota(jnp.int32, (4, 1024), 0) + (ring(z, off) * RING + y) * 4).astype(F32)
        for h in range(2):
            hit = jnp.zeros((4, 1024), F32)
            for s in range(SEL):
                hit = jnp.where(block == lists[h][s : s + 1, :], 1.0, hit)
            hit = jnp.where(block < own_id, hit, 0.0)
            hit = jnp.where(block == own_id, 1.0, hit)
            bias[h, i] = jnp.where(hit > 0.5, 0.0, MASKED)

    head0 = lax.broadcasted_iota(jnp.int32, (TOK, COLS), 1) < HD
    zero = jnp.zeros((TOK, COLS), BF16)

    def stage(i):
        for src, dst in ((first, qm), (second, gm)):
            tile = qg[i, src, :]
            dst[i, first, :] = jnp.where(head0, tile, zero)
            dst[i, second, :] = jnp.where(head0, zero, tile)
        kt[:, i * TOK : (i + 1) * TOK] = kv[i, first, :].astype(F32).T.astype(BF16)

    row_i = lax.broadcasted_iota(jnp.int32, (TOK, TOK), 0)
    col_i = lax.broadcasted_iota(jnp.int32, (TOK, TOK), 1)
    future = (row_i // BLK == col_i // BLK) & (row_i > col_i)
    diag_bias = jnp.where(future, MASKED, 0.0).astype(F32)
    for h in range(2):
        da[h] = jnp.zeros((8, 8, TOK), F32)

    def strip(i, columns, diagonal=False):
        k_tile = kv[i, first, :]
        v_tile = kv[i, second, :]
        for j in columns:
            s = nt(k_tile, qm[j])
            dp = nt(v_tile, gm[j])
            for h in range(2):
                lanes = slice(h * TOK, (h + 1) * TOK)
                rows = bias[h, i, :, j * TOK : (j + 1) * TOK] - ls[j, h : h + 1, :]
                rows = jnp.concatenate(
                    [jnp.broadcast_to(rows[b : b + 1], (BLK, TOK)) for b in range(4)], axis=0
                )
                x = s[:, lanes] * 0.125 + rows
                if diagonal:
                    x = x + diag_bias
                w = jnp.exp(x)
                d = dp[:, lanes]
                at = j * 256 + h * TOK
                wf[i, :, at : at + TOK] = w
                dpf[i, :, at : at + TOK] = d
                w16[i, :, at : at + TOK] = w.astype(BF16)
                da[h, j] += jnp.sum((w * d).reshape(16, 8, TOK), axis=0)

    def strips(lo, hi, columns):
        def one(i, _):
            strip(i, columns)
            return 0

        lax.fori_loop(lo, hi, one, 0)

    stage(0)
    strip(0, (0,), True)

    def wait_group(r, n, ref):
        remote(ref, ref, done.at[r[3]], r[2].at[n], r[1](1)).wait_recv()

    for half, r, d in steps:
        buf = r[0]
        wait_group(r, group(-2 * d, half), buf.at[slot(-2 * d), halves[half]])
        if half == (d < 0):
            pass_on(r, -2 * d, half, 2 * d)
        pass_on(r, -2 * d, half, d)
    remote(ls.at[pl.ds(1, 7)], ls.at[pl.ds(1, 7)], done.at[2], come.at[2], along_y(1)).wait_recv()
    stage(1)
    stage(2)
    strips(1, 3, (0, 1, 2))
    strip(0, (1, 2))
    for r in rings:
        wait_group(r, 4, r[0].at[pl.ds(3, 2)])
    stage(3)
    stage(4)
    strips(3, 5, (0, 1, 2, 3, 4))
    strips(0, 3, (3, 4))
    for r in rings:
        wait_group(r, 5, r[0].at[pl.ds(5, 2)])
    stage(5)
    stage(6)
    strips(5, 7, (0, 1, 2, 3, 4, 5, 6))
    strips(0, 5, (5, 6))
    for r in rings:
        wait_group(r, 6, r[0].at[7])
    stage(7)
    strip(7, (0, 1, 2, 3, 4, 5, 6, 7))
    strips(0, 7, (7,))

    for j, off in enumerate(ORDER):
        for h in range(2):
            dl[0, ring(y, off), h : h + 1, :] = jnp.sum(da[h, j], axis=0, keepdims=True)
    for off in FAR:
        remote(dl.at[0], dl.at[slot(-off)], done.at[4], come.at[4], along_y(off)).start()

    def value_grad(i, _):
        dvs[i] = nn(w16[i], gm[...].reshape(2048, COLS)).astype(BF16)
        return 0

    lax.fori_loop(0, RING, value_grad, 0)
    for off in FAR:
        remote(dvs.at[slot(off)], dvr.at[slot(-off)], done.at[5], come.at[5], along_z(off)).start()

    rest = pl.ds(1, 7)
    remote(xg.at[rest], xg.at[rest], done.at[3], come.at[3], along_tp(1)).wait_recv()
    for o in range(RING):
        xt[pl.ds(pl.multiple_of(ring(tp, o) * 256, 256), 256), :] = xg[o].astype(F32).T.astype(BF16)

    remote(dl.at[rest], dl.at[rest], done.at[4], come.at[4], along_y(1)).wait_recv()

    for off in FAR + (0,):
        j = slot(off)
        total = dl[0, ring(y, off)]
        for n in range(1, RING):
            total = total + dl[n, ring(y, off)]

        def score_grad(i, _, j=j, total=total):
            for h in range(2):
                at = j * 256 + h * TOK
                ds16[i, :, at : at + TOK] = (
                    wf[i, :, at : at + TOK] * (dpf[i, :, at : at + TOK] - total[h : h + 1, :])
                ).astype(BF16)
            return 0

        lax.fori_loop(0, RING, score_grad, 0, unroll=2)
        both = nn(kt[...], ds16[:, :, j * 256 : (j + 1) * 256].reshape(1024, 256))
        dqs[j, 0:HD, :] = both[0:HD, 0:TOK].astype(BF16)
        dqs[j, HD:COLS, :] = both[HD:COLS, TOK:256].astype(BF16)
        if off:
            remote(dqs.at[j], dqr.at[slot(-off)], done.at[6], come.at[6], along_y(off)).start()

    def key_grad(i, _):
        dks[i] = nn(ds16[i], qm[...].reshape(2048, COLS)).astype(BF16)
        return 0

    lax.fori_loop(0, RING, key_grad, 0)
    for off in FAR:
        remote(dks.at[slot(off)], dkr.at[slot(-off)], done.at[7], come.at[7], along_z(off)).start()

    def summed(own, arrived, n, along):
        remote(arrived.at[rest], arrived.at[rest], done.at[n], come.at[n], along(1)).wait_recv()
        acc = own.astype(F32)
        for i in range(1, RING):
            acc = acc + arrived[i].astype(F32)
        return acc

    dq = (summed(dqs[0], dqr, 6, along_y) * 0.125).T.astype(BF16)
    dq_out[...] = dq

    def weight_part(zz, _):
        part = nn(xt[pl.ds(pl.multiple_of(zz * 256, 256), 256), :], dq)
        part = part.astype(BF16).reshape(RING, 2, 16, COLS)
        gas[zz] = part[:, 0]
        gbs[:, zz] = part[:, 1]
        return 0

    lax.fori_loop(0, RING, weight_part, 0)
    for off in FAR:
        remote(gas.at[ring(z, off)], gar.at[slot(-off)], done.at[8], come.at[8], along_z(off)).start()
        remote(gbs.at[ring(y, off)], gbr.at[slot(-off)], done.at[9], come.at[9], along_y(off)).start()

    dv_out[...] = summed(dvs[0], dvr, 5, along_z).astype(BF16)
    dk_out[...] = (summed(dks[0], dkr, 7, along_z) * 0.125).astype(BF16)

    ha_s[...] = summed(gas[z], gar, 8, along_z).astype(BF16)
    for off in FAR:
        remote(ha_s.at[ring(y, off)], ha_r.at[slot(-off)], done.at[10], come.at[10], along_y(off)).start()
    hb_s[...] = summed(gbs[y], gbr, 9, along_y).astype(BF16)
    for off in FAR:
        remote(hb_s.at[ring(z, off)], hb_r.at[slot(-off)], done.at[11], come.at[11], along_z(off)).start()
    gw_out[0:16, :] = summed(ha_s[y], ha_r, 10, along_y)
    gw_out[16:32, :] = summed(hb_s[z], hb_r, 11, along_z)

    for n, ref in enumerate((qg, kv, ls, xg, dl, dvs, dqs, dks, gas, gbs, ha_s, hb_s)):
        part = ref.at[rest]
        remote(part, part, done.at[n], come.at[n], along_y(1)).wait_send()


def body(queries, keys, values, cotangent, log_sum, chosen, normed_input):
    vm = pltpu.VMEM
    dma = pltpu.SemaphoreType.DMA
    scratch = [
        vm((8, 256, 128), BF16),
        vm((8, 256, 128), BF16),
        vm((8, 2, 128), F32),
        vm((8, 128, 256), BF16),
        vm((SEL, 2, 256), jnp.int32),
        vm((8, 256, 128), BF16),
        vm((8, 256, 128), BF16),
        vm((128, 1024), BF16),
        vm((2048, 128), BF16),
        vm((2, 8, 4, 1024), F32),
        vm((8, 128, 2048), F32),
        vm((8, 128, 2048), F32),
        vm((8, 128, 2048), BF16),
        vm((8, 128, 2048), BF16),
        vm((2, 8, 8, 128), F32),
        vm((8, 8, 2, 128), F32),
    ]
    scratch += [vm((8, 128, 128), BF16)] * 6
    scratch += [vm((8, 8, 16, 128), BF16)] * 4
    scratch += [vm((8, 16, 128), BF16)] * 4
    scratch += [dma((7,)), dma((7,)), dma((7,)), dma((12,)), dma((12,))]
    return pl.pallas_call(
        kernel,
        out_shape=(
            jax.ShapeDtypeStruct((TOK, COLS), BF16),
            jax.ShapeDtypeStruct((TOK, COLS), BF16),
            jax.ShapeDtypeStruct((TOK, COLS), BF16),
            jax.ShapeDtypeStruct((32, COLS), F32),
        ),
        in_specs=[pl.BlockSpec(memory_space=pl.ANY)] * 7,
        out_specs=[pl.BlockSpec(memory_space=pltpu.VMEM)] * 4,
        scratch_shapes=scratch,
        compiler_params=pltpu.CompilerParams(
            collective_id=0, has_side_effects=True, vmem_limit_bytes=60 * 1024 * 1024
        ),
    )(queries, keys, values, cotangent, log_sum, chosen.transpose(2, 0, 1), normed_input)


def solution(mesh):
    in_specs = (
        P("kv", "tp"),
        P("kv", "tp"),
        P("kv", "tp"),
        P("kv", "tp"),
        P("tp", "kv"),
        P("tp", None, None),
        P("kv", "tp"),
    )
    out_specs = (P("kv", "tp"), P("kv", "tp"), P("kv", "tp"), P("kv", "tp"))
    return jax.shard_map(body, mesh=mesh, in_specs=in_specs, out_specs=out_specs, check_vma=False)
```

time: 73.6 us -> 61.2 us (0.83)
  Pallas kernels: 67.2 us -> 56 us
  local copies, waits for them, and re-layouts: 5.06 us -> 3.49 us
    pallas_call x1, Pallas kernels: 67.2 us -> 56 us  [body(): pl.pallas_call(kernel, out_shape=(jax.ShapeDtypeStruct((TOK, COLS), BF16)...]
    unnamed x11 -> x10, local copies, waits for them, and re-layouts: 5.06 us -> 3.49 us
where the time goes in v2:
time: 61.2 us; the launch traced here: 60.1 us
  Pallas kernels  56 us (92%)
  local copies, waits for them, and re-layouts  3.49 us (6%)
  between operations  0.65 us (1%)
    pallas_call x1, Pallas kernels, body(): pl.pallas_call(kernel, out_shape=(jax.ShapeDtypeStruct((TOK, COLS), BF16)...  56 us
    unnamed x10, local copies, waits for them, and re-layouts  3.49 us

profile of v2, /device:TPU:6, one launch (start us, length us, event | category | flops | bytes accessed | tf_op | source)
XLA Modules:
  0.0 60.1 jit_solution(10867351512205529478)
XLA Ops:
  0.6 56.0 %shard_map.102 = (bf16[128,128]{1,0:T(8,128)(2,1)}, bf16[128,128]{1,0:T(8,128)(2,1)}, bf16[128,128]{1,0:T(8,128)(2,1)}, f32[32,128]{1,0:T(8,128)}) custom-call(bf16[128,128]{1,0:T(8,128)(2,1)} %q_in.1, bf16[128,128]{1,0:T(8,128)(2,1)} %k_in.1, bf16[128,128]{1,0:T(8,128)(2,1)} %v_in.1, bf16[128,128]{1,0:T(8,128)(2,1)} %g_in.1, f32[2,128]{1,0:T(2,128)} %ls_in.1, ...), custom_call_target="tpu_custom_call" | custom-call | tf_op jit(solution)/shard_map/pallas_call | solution.py:323
  56.6 0.0 copy-start.1
  56.6 1.4 %copy.15 = bf16[128,128]{1,0:T(8,128)(2,1)} copy(bf16[128,128]{1,0:T(8,128)(2,1)} %get-tuple-element.8) | data formatting | bytes 65536
  58.0 0.0 copy-done.1
  58.0 0.0 copy-start
  58.0 0.6 %copy.16 = bf16[128,128]{1,0:T(8,128)(2,1)} copy(bf16[128,128]{1,0:T(8,128)(2,1)S(1)} %copy-done.1) | data formatting | bytes 65536
  58.6 0.2 copy-done
  58.8 0.0 copy-start.2
  58.8 0.6 %copy.17 = bf16[128,128]{1,0:T(8,128)(2,1)} copy(bf16[128,128]{1,0:T(8,128)(2,1)S(1)} %copy-done) | data formatting | bytes 65536
  59.4 0.1 copy-done.2
  59.5 0.6 %copy.18 = f32[32,128]{1,0:T(8,128)} copy(f32[32,128]{1,0:T(8,128)S(1)} %copy-done.2) | data formatting | bytes 32768
Async XLA Ops:
  56.6 1.4 %copy-start.1 = (bf16[128,128]{1,0:T(8,128)(2,1)S(1)}, bf16[128,128]{1,0:T(8,128)(2,1)}, u32[]{:S(2)}) copy-start(bf16[128,128]{1,0:T(8,128)(2,1)} %get-tuple-element.9) | copy-start | bytes 98308
  58.0 0.8 %copy-start = (bf16[128,128]{1,0:T(8,128)(2,1)S(1)}, bf16[128,128]{1,0:T(8,128)(2,1)}, u32[]{:S(2)}) copy-start(bf16[128,128]{1,0:T(8,128)(2,1)} %get-tuple-element.10) | copy-start | bytes 98308
  58.8 0.7 %copy-start.2 = (f32[32,128]{1,0:T(8,128)S(1)}, f32[32,128]{1,0:T(8,128)}, u32[]{:S(2)}) copy-start(f32[32,128]{1,0:T(8,128)} %get-tuple-element.11) | copy-start | bytes 49156

commit v3 on v2

v3 whole, which is shorter than its diff:
```python
import jax
import jax.numpy as jnp
from jax import lax
from jax.experimental import pallas as pl
from jax.experimental.pallas import tpu as pltpu
from jax.sharding import PartitionSpec as P

HD = 64
BLK = 32
SEL = 12
MASKED = -1e30
RING = 8
TOK = 128
COLS = 128
ORDER = (0, 2, -2, 1, -1, 3, -3, 4)
POS = {off % RING: i for i, off in enumerate(ORDER)}
FAR = (4, 3, -3, 2, -2, 1, -1)
MESH = pl.DeviceIdType.MESH
F32 = jnp.float32
BF16 = jnp.bfloat16


def nt(a, b):
    return lax.dot_general(a, b, (((1,), (1,)), ((), ())), preferred_element_type=F32)


def nn(a, b):
    return lax.dot_general(a, b, (((1,), (0,)), ((), ())), preferred_element_type=F32)


def kernel(
    q_in, k_in, v_in, g_in, ls_in, ch_in, x_in,
    dq_out, dk_out, dv_out, gw_out,
    raw, qg, kv, ls, xg, chs, qmt, gmt, kt, xt, bias, wf, dpf, w16, ds16, da, dl, tot,
    dvs, dvr, dks, dkr, dqs, dqr, gas, gar, gbs, gbr, ha_s, ha_r, hb_s, hb_r,
    loc, gather, done, come,
):
    me = lax.axis_index("kv")
    tp = lax.axis_index("tp")
    z = me // RING
    y = me % RING

    def ring(base, off):
        return (base + off + RING) % RING

    def dev(axis, off):
        return z * RING + ring(y, off) if axis == 0 else ring(z, off) * RING + y

    def along(axis, off):
        return (dev(axis, off), tp)

    def remote(src, dst, send, recv, target):
        return pltpu.make_async_remote_copy(
            src_ref=src, dst_ref=dst, send_sem=send, recv_sem=recv, device_id=target, device_id_type=MESH
        )

    def slot(off):
        return POS[off % RING]

    barrier = pltpu.get_barrier_semaphore()
    for off in range(1, RING):
        for target in (along(0, off), along(1, off), (me, ring(tp, off))):
            pl.semaphore_signal(barrier, inc=1, device_id=target, device_id_type=MESH)

    loads = [
        pltpu.make_async_copy(src, dst, loc.at[n])
        for n, (src, dst) in enumerate(
            (
                (q_in, raw.at[0]), (g_in, raw.at[1]), (k_in, raw.at[2]), (v_in, raw.at[3]),
                (ls_in, ls.at[0, 0]), (ls_in, ls.at[1, 0]), (x_in, xg.at[0]), (ch_in, chs),
            )
        )
    ]
    for c in loads:
        c.start()
    left = lax.broadcasted_iota(jnp.int32, (TOK, COLS), 1) < HD
    for n, buf in ((0, qg), (2, kv)):
        loads[n].wait()
        loads[n + 1].wait()
        a, b = raw[n].astype(F32), raw[n + 1].astype(F32)
        buf[0, 0] = jnp.where(left, a, pltpu.roll(b, HD, 1)).astype(BF16)
        buf[1, 0] = jnp.where(left, pltpu.roll(a, HD, 1), b).astype(BF16)
    for c in loads[4:]:
        c.wait()
    pl.semaphore_wait(barrier, 3 * (RING - 1))

    def piece(axis, half):
        return qg.at[axis] if half == 0 else kv.at[1 - axis]

    steps = [(half, axis, d) for half in (0, 1) for axis in (0, 1) for d in (1, -1)]

    def group(off, half):
        near = (off + 4) % RING - 4
        if abs(near) == 2:
            return (0 if near < 0 else 2) + half
        return {1: 4, 3: 6, 4: 8}[abs(near)] + half

    def pass_on(axis, src, half, hop):
        buf = piece(axis, half)
        remote(
            buf.at[slot(src)],
            buf.at[slot(src - hop)],
            done.at[2 * axis + half],
            gather.at[axis, group(src - hop, half)],
            along(axis, hop),
        ).start()

    for half, axis, d in steps:
        pass_on(axis, 0, half, 2 * d)
    for half, axis, d in steps:
        pass_on(axis, 0, half, d)
    for off in FAR:
        for axis in (0, 1):
            remote(
                ls.at[axis, 0], ls.at[axis, slot(-off)], done.at[4 + axis], come.at[4 + axis], along(axis, off)
            ).start()
    for off in range(1, RING):
        remote(xg.at[0], xg.at[RING - off], done.at[6], come.at[6], (me, ring(tp, off))).start()

    lane = lax.broadcasted_iota(jnp.int32, (1, TOK), 1) // BLK
    for h in range(2):
        own_id = jnp.concatenate([dev(h, off) * 4 + lane for off in ORDER], axis=1)
        spread = (lax.broadcasted_iota(jnp.int32, (256, 1024), 0) == own_id).astype(BF16)
        own_id = own_id.astype(F32)
        lists = nn(chs[:, h, :].astype(F32).astype(BF16), spread)
        for i, off in enumerate(ORDER):
            block = (lax.broadcasted_iota(jnp.int32, (4, 1024), 0) + dev(1 - h, off) * 4).astype(F32)
            hit = jnp.zeros((4, 1024), F32)
            for s in range(SEL):
                hit = jnp.where(block == lists[s : s + 1, :], 1.0, hit)
            hit = jnp.where(block < own_id, hit, 0.0)
            hit = jnp.where(block == own_id, 1.0, hit)
            bias[h, i] = jnp.where(hit > 0.5, 0.0, MASKED)

    for h in range(2):
        qmt[h, HD:COLS, :] = jnp.zeros((HD, 1024), BF16)
        gmt[h, 0:HD, :] = jnp.zeros((HD, 1024), BF16)
        da[h] = jnp.zeros((8, 8, TOK), F32)

    def stage(i):
        lanes = slice(i * TOK, (i + 1) * TOK)
        for h in range(2):
            turned = qg[h, i].astype(F32).T.astype(BF16)
            qmt[h, 0:HD, lanes] = turned[0:HD]
            gmt[h, HD:COLS, lanes] = turned[HD:COLS]
            kt[h, :, lanes] = kv[h, i].astype(F32).T[0:HD].astype(BF16)

    row_i = lax.broadcasted_iota(jnp.int32, (TOK, TOK), 0)
    col_i = lax.broadcasted_iota(jnp.int32, (TOK, TOK), 1)
    future = (row_i // BLK == col_i // BLK) & (row_i > col_i)
    diag_bias = jnp.where(future, MASKED, 0.0).astype(F32)

    def strip(i, lo, hi, diagonal=False):
        for h in range(2):
            tile = kv[h, i]
            for at in range(lo, hi, 2):
                end = min(at + 2, hi)
                s = nn(tile, qmt[h, :, at * TOK : end * TOK])
                dp = nn(tile, gmt[h, :, at * TOK : end * TOK])
                for j in range(at, end):
                    lanes = slice((j - at) * TOK, (j - at + 1) * TOK)
                    into = slice(j * TOK, (j + 1) * TOK)
                    rows = bias[h, i, :, into] - ls[h, j, h : h + 1, :]
                    rows = jnp.concatenate(
                        [jnp.broadcast_to(rows[b : b + 1], (BLK, TOK)) for b in range(4)], axis=0
                    )
                    x = s[:, lanes] * 0.125 + rows
                    if diagonal:
                        x = x + diag_bias
                    w = jnp.exp(x)
                    d = dp[:, lanes]
                    wf[h, i, :, into] = w
                    dpf[h, i, :, into] = d
                    w16[h, i, :, into] = w.astype(BF16)
                    da[h, j] += jnp.sum((w * d).reshape(16, 8, TOK), axis=0)

    def strips(first, last, lo, hi, unroll=1):
        def one(i, _):
            strip(i, lo, hi)
            return 0

        lax.fori_loop(first, last, one, 0, unroll=unroll)

    stage(0)
    strip(0, 0, 1, True)

    def arrive(axis, n, ref):
        remote(ref, ref, done.at[2 * axis], gather.at[axis, n], along(axis, 1)).wait_recv()

    rest = pl.ds(1, 7)
    for half, axis, d in steps:
        arrive(axis, group(-2 * d, half), piece(axis, half).at[slot(-2 * d)])
        if half == (d < 0):
            pass_on(axis, -2 * d, half, 2 * d)
        pass_on(axis, -2 * d, half, d)
    for axis in (0, 1):
        part = ls.at[axis, rest]
        remote(part, part, done.at[4 + axis], come.at[4 + axis], along(axis, 1)).wait_recv()
    stage(1)
    stage(2)
    strips(1, 3, 0, 3)
    strip(0, 1, 3)
    for n, first in ((4, 3), (6, 5)):
        for axis in (0, 1):
            for half in (0, 1):
                arrive(axis, n + half, piece(axis, half).at[pl.ds(first, 2)])
        stage(first)
        stage(first + 1)
        strips(first, first + 2, 0, first + 2)
        strips(0, first, first, first + 2)
    for axis in (0, 1):
        for half in (0, 1):
            arrive(axis, 8 + half, piece(axis, half).at[7])
    stage(7)
    strip(7, 0, 8)
    strips(0, 7, 7, 8, unroll=7)

    for axis in (0, 1):
        for j, off in enumerate(ORDER):
            row = ring(y if axis == 0 else z, off)
            dl[axis, 0, pl.ds(row, 1), :] = jnp.sum(da[axis, j], axis=0, keepdims=True)
    for off in FAR:
        for axis in (0, 1):
            remote(
                dl.at[axis, 0], dl.at[axis, slot(-off)], done.at[7 + axis], come.at[7 + axis], along(axis, off)
            ).start()

    def scatter(buf, into, h, axis, n):
        for off in FAR:
            remote(
                buf.at[h, slot(off)], into.at[h, slot(-off)], done.at[n + h], come.at[n + h], along(axis, off)
            ).start()

    def value_grad(i, _):
        for h in range(2):
            dvs[h, i] = nt(gmt[h, HD:COLS, :], w16[h, i]).astype(BF16)
        return 0

    lax.fori_loop(0, RING, value_grad, 0)
    for h in range(2):
        scatter(dvs, dvr, h, 1 - h, 9)

    part = xg.at[rest]
    remote(part, part, done.at[6], come.at[6], (me, ring(tp, 1))).wait_recv()
    for o in range(RING):
        xt[pl.ds(pl.multiple_of(ring(tp, o) * 256, 256), 256), :] = xg[o].astype(F32).T.astype(BF16)

    for axis in (0, 1):
        part = dl.at[axis, rest]
        remote(part, part, done.at[7 + axis], come.at[7 + axis], along(axis, 1)).wait_recv()
        acc = dl[axis, 0]
        for n in range(1, RING):
            acc = acc + dl[axis, n]
        tot[axis] = acc

    for off in FAR + (0,):
        j = slot(off)
        into = slice(j * TOK, (j + 1) * TOK)
        for h in range(2):
            delta = tot[h, pl.ds(ring(y if h == 0 else z, off), 1), :]

            def score_grad(i, _, h=h, into=into, delta=delta):
                ds16[h, i, :, into] = (wf[h, i, :, into] * (dpf[h, i, :, into] - delta)).astype(BF16)
                return 0

            lax.fori_loop(0, RING, score_grad, 0, unroll=4)
            dqs[h, j] = nn(kt[h], ds16[h, :, :, into].reshape(1024, TOK)).astype(BF16)
            if off:
                remote(
                    dqs.at[h, j], dqr.at[h, slot(-off)], done.at[11 + h], come.at[11 + h], along(h, off)
                ).start()

    def key_grad(i, _):
        for h in range(2):
            dks[h, i] = nt(qmt[h, 0:HD, :], ds16[h, i]).astype(BF16)
        return 0

    lax.fori_loop(0, RING, key_grad, 0)
    for h in range(2):
        scatter(dks, dkr, h, 1 - h, 13)

    def both_heads(own, arrived, n):
        sums = []
        for h in range(2):
            part = arrived.at[h, rest]
            remote(part, part, done.at[n + h], come.at[n + h], along(0, 1)).wait_recv()
            acc = own[h, 0].astype(F32)
            for i in range(1, RING):
                acc = acc + arrived[h, i].astype(F32)
            sums.append(acc)
        return jnp.concatenate(sums, axis=0).T

    dq = (both_heads(dqs, dqr, 11) * 0.125).astype(BF16)
    dq_out[...] = dq

    def weight_part(zz, _):
        part = nn(xt[pl.ds(pl.multiple_of(zz * 256, 256), 256), :], dq)
        part = part.astype(BF16).reshape(RING, 2, 16, COLS)
        gas[zz] = part[:, 0]
        gbs[:, zz] = part[:, 1]
        return 0

    lax.fori_loop(0, RING, weight_part, 0, unroll=4)
    for off in FAR:
        remote(gas.at[ring(z, off)], gar.at[slot(-off)], done.at[15], come.at[15], along(1, off)).start()
        remote(gbs.at[ring(y, off)], gbr.at[slot(-off)], done.at[16], come.at[16], along(0, off)).start()

    dv_out[...] = both_heads(dvs, dvr, 9).astype(BF16)
    dk_out[...] = (both_heads(dks, dkr, 13) * 0.125).astype(BF16)

    def summed(own, arrived, n):
        part = arrived.at[rest]
        remote(part, part, done.at[n], come.at[n], along(0, 1)).wait_recv()
        acc = own.astype(F32)
        for i in range(1, RING):
            acc = acc + arrived[i].astype(F32)
        return acc

    ha_s[...] = summed(gas[z], gar, 15).astype(BF16)
    for off in FAR:
        remote(ha_s.at[ring(y, off)], ha_r.at[slot(-off)], done.at[17], come.at[17], along(0, off)).start()
    hb_s[...] = summed(gbs[y], gbr, 16).astype(BF16)
    for off in FAR:
        remote(hb_s.at[ring(z, off)], hb_r.at[slot(-off)], done.at[18], come.at[18], along(1, off)).start()
    gw_out[0:16, :] = summed(ha_s[y], ha_r, 17)
    gw_out[16:32, :] = summed(hb_s[z], hb_r, 18)

    sent = [qg.at[0, rest], kv.at[1, rest], qg.at[1, rest], kv.at[0, rest], ls.at[0, rest], ls.at[1, rest]]
    sent += [xg.at[rest], dl.at[0, rest], dl.at[1, rest]]
    sent += [buf.at[h, rest] for buf in (dvs, dqs, dks) for h in range(2)]
    sent += [buf.at[rest] for buf in (gas, gbs, ha_s, hb_s)]
    for n, part in enumerate(sent):
        remote(part, part, done.at[n], come.at[n], along(0, 1)).wait_send()


def write_out(a, b, c, d, a_out, b_out, c_out, d_out, sems):
    copies = [
        pltpu.make_async_copy(src, dst, sems.at[n])
        for n, (src, dst) in enumerate(((a, a_out), (b, b_out), (c, c_out), (d, d_out)))
    ]
    for copy in copies:
        copy.start()
    for copy in copies:
        copy.wait()


def body(queries, keys, values, cotangent, log_sum, chosen, normed_input):
    vm = pltpu.VMEM
    dma = pltpu.SemaphoreType.DMA
    scratch = [
        vm((4, 128, 128), BF16),
        vm((2, 8, 128, 128), BF16),
        vm((2, 8, 128, 128), BF16),
        vm((2, 8, 2, 128), F32),
        vm((8, 128, 256), BF16),
        vm((SEL, 2, 256), jnp.int32),
        vm((2, 128, 1024), BF16),
        vm((2, 128, 1024), BF16),
        vm((2, 64, 1024), BF16),
        vm((2048, 128), BF16),
        vm((2, 8, 4, 1024), F32),
        vm((2, 8, 128, 1024), F32),
        vm((2, 8, 128, 1024), F32),
        vm((2, 8, 128, 1024), BF16),
        vm((2, 8, 128, 1024), BF16),
        vm((2, 8, 8, 128), F32),
        vm((2, 8, 8, 128), F32),
        vm((2, 8, 128), F32),
    ]
    scratch += [vm((2, 8, 64, 128), BF16)] * 6
    scratch += [vm((8, 8, 16, 128), BF16)] * 4
    scratch += [vm((8, 16, 128), BF16)] * 4
    scratch += [dma((8,)), dma((2, 10)), dma((19,)), dma((19,))]
    shapes = (
        jax.ShapeDtypeStruct((TOK, COLS), BF16),
        jax.ShapeDtypeStruct((TOK, COLS), BF16),
        jax.ShapeDtypeStruct((TOK, COLS), BF16),
        jax.ShapeDtypeStruct((32, COLS), F32),
    )
    inside = pl.pallas_call(
        kernel,
        out_shape=shapes,
        in_specs=[pl.BlockSpec(memory_space=pl.ANY)] * 7,
        out_specs=[pl.BlockSpec(memory_space=pltpu.VMEM)] * 4,
        scratch_shapes=scratch,
        compiler_params=pltpu.CompilerParams(
            collective_id=0, has_side_effects=True, vmem_limit_bytes=55080 * 1024
        ),
    )(queries, keys, values, cotangent, log_sum, chosen.transpose(2, 0, 1), normed_input)
    return pl.pallas_call(
        write_out,
        out_shape=shapes,
        in_specs=[pl.BlockSpec(memory_space=pltpu.VMEM)] * 4,
        out_specs=[pl.BlockSpec(memory_space=pl.ANY)] * 4,
        scratch_shapes=[dma((4,))],
        compiler_params=pltpu.CompilerParams(vmem_limit_bytes=4 * 1024 * 1024),
    )(*inside)


def solution(mesh):
    in_specs = (
        P("kv", "tp"),
        P("kv", "tp"),
        P("kv", "tp"),
        P("kv", "tp"),
        P("tp", "kv"),
        P("tp", None, None),
        P("kv", "tp"),
    )
    out_specs = (P("kv", "tp"), P("kv", "tp"), P("kv", "tp"), P("kv", "tp"))
    return jax.shard_map(body, mesh=mesh, in_specs=in_specs, out_specs=out_specs, check_vma=False)
```

time: 61.2 us -> 57.9 us (0.946)
  local copies, waits for them, and re-layouts: 3.49 us -> 1.41 us
  Pallas kernels: 56 us -> 55.3 us
    unnamed x10 -> x4, local copies, waits for them, and re-layouts: 3.49 us -> 1.41 us
    pallas_call x1 -> x2, Pallas kernels: 56 us -> 55.3 us  [the longest x1 54.6 us: body(): pl.pallas_call(kernel, out_shape=shapes, in_specs=[pl.BlockSpec(memory_sp...]
where the time goes in v3:
time: 57.9 us; the launch traced here: 57.3 us
  Pallas kernels  55.3 us (96%)
  local copies, waits for them, and re-layouts  1.41 us (2%)
  between operations  0.65 us (1%)
    pallas_call x1, Pallas kernels, body(): pl.pallas_call(kernel, out_shape=shapes, in_specs=[pl.BlockSpec(memory_sp...  54.6 us
    unnamed x4, local copies, waits for them, and re-layouts  1.41 us

profile of v3, /device:TPU:6, one launch (start us, length us, event | category | flops | bytes accessed | tf_op | source)
XLA Modules:
  0.0 57.3 jit_solution(11081010662702700276)
XLA Ops:
  0.6 0.0 copy-start.1
  0.6 0.7 %copy-done.1 = f32[2,128]{1,0:T(2,128)S(1)} copy-done((f32[2,128]{1,0:T(2,128)S(1)}, f32[2,128]{1,0:T(2,128)}, u32[]{:S(2)}) %copy-start.1) | copy-done | bytes 1048
  1.3 0.0 copy-start
  1.3 0.7 %copy-done = s32[2,256,12]{1,0,2:T(2,128)S(1)} copy-done((s32[2,256,12]{1,0,2:T(2,128)S(1)}, s32[2,256,12]{1,0,2:T(2,128)}, u32[]{:S(2)}) %copy-start) | copy-done | bytes 24600
  2.1 54.6 %shard_map.102 = (bf16[128,128]{1,0:T(8,128)(2,1)S(1)}, bf16[128,128]{1,0:T(8,128)(2,1)S(1)}, bf16[128,128]{1,0:T(8,128)(2,1)S(1)}, f32[32,128]{1,0:T(8,128)S(1)}) custom-call(bf16[128,128]{1,0:T(8,128)(2,1)} %q_in.1, bf16[128,128]{1,0:T(8,128)(2,1)} %k_in.1, bf16[128,128]{1,0:T(8,128)(2,1)} %v_in.1, bf16[128,128]{1,0:T(8,128)(2,1)} %g_in.1, ...), custom_call_target="tpu_custom_call" | custom-call | tf_op jit(solution)/shard_map/pallas_call | solution.py:380
  56.7 0.7 %shard_map.103 = (bf16[128,128]{1,0:T(8,128)(2,1)}, bf16[128,128]{1,0:T(8,128)(2,1)}, bf16[128,128]{1,0:T(8,128)(2,1)}, f32[32,128]{1,0:T(8,128)}) custom-call(bf16[128,128]{1,0:T(8,128)(2,1)S(1)} %get-tuple-element.8.a, bf16[128,128]{1,0:T(8,128)(2,1)S(1)} %get-tuple-element.9.b, bf16[128,128]{1,0:T(8,128)(2,1)S(1)} %get-tuple-element.10.c, ...), custom_call_target="tpu_custom_call" | custom-call | tf_op jit(solution)/shard_map/pallas_call | solution.py:390
Async XLA Ops:
  0.6 0.7 %copy-start.1 = (f32[2,128]{1,0:T(2,128)S(1)}, f32[2,128]{1,0:T(2,128)}, u32[]{:S(2)}) copy-start(f32[2,128]{1,0:T(2,128)} %ls_in.1) | copy-start | bytes 3076
  1.3 0.7 %copy-start = (s32[2,256,12]{1,0,2:T(2,128)S(1)}, s32[2,256,12]{1,0,2:T(2,128)}, u32[]{:S(2)}) copy-start(s32[2,256,12]{1,0,2:T(2,128)} %param.12) | copy-start | bytes 73732

commit v4 on v3

--- a/solution.py
+++ b/solution.py
@@ -236,7 +236,7 @@
             dvs[h, i] = nt(gmt[h, HD:COLS, :], w16[h, i]).astype(BF16)
         return 0
 
-    lax.fori_loop(0, RING, value_grad, 0)
+    lax.fori_loop(0, RING, value_grad, 0, unroll=4)
     for h in range(2):
         scatter(dvs, dvr, h, 1 - h, 9)
 
@@ -253,21 +253,26 @@
             acc = acc + dl[axis, n]
         tot[axis] = acc
 
-    for off in FAR + (0,):
-        j = slot(off)
-        into = slice(j * TOK, (j + 1) * TOK)
-        for h in range(2):
-            delta = tot[h, pl.ds(ring(y if h == 0 else z, off), 1), :]
-
-            def score_grad(i, _, h=h, into=into, delta=delta):
-                ds16[h, i, :, into] = (wf[h, i, :, into] * (dpf[h, i, :, into] - delta)).astype(BF16)
-                return 0
-
-            lax.fori_loop(0, RING, score_grad, 0, unroll=4)
-            dqs[h, j] = nn(kt[h], ds16[h, :, :, into].reshape(1024, TOK)).astype(BF16)
-            if off:
+    for lo, hi in ((7, 8), (5, 7), (1, 3), (3, 5), (0, 1)):
+        into = slice(lo * TOK, hi * TOK)
+        for h in range(2):
+            delta = jnp.concatenate(
+                [tot[h, pl.ds(ring(y if h == 0 else z, ORDER[j]), 1), :] for j in range(lo, hi)], axis=1
+            )
+            acc = jnp.zeros((HD, (hi - lo) * TOK), F32)
+            for i in range(0, RING, 2):
+                pair = []
+                for n in (i, i + 1):
+                    low = (wf[h, n, :, into] * (dpf[h, n, :, into] - delta)).astype(BF16)
+                    ds16[h, n, :, into] = low
+                    pair.append(low)
+                acc = acc + nn(kt[h, :, i * TOK : (i + 2) * TOK], jnp.concatenate(pair, axis=0))
+            for j in range(lo, hi):
+                dqs[h, j] = acc[:, (j - lo) * TOK : (j - lo + 1) * TOK].astype(BF16)
+        for j in range(max(lo, 1), hi):
+            for h in range(2):
                 remote(
-                    dqs.at[h, j], dqr.at[h, slot(-off)], done.at[11 + h], come.at[11 + h], along(h, off)
+                    dqs.at[h, j], dqr.at[h, slot(-ORDER[j])], done.at[11 + h], come.at[11 + h], along(h, ORDER[j])
                 ).start()
 
     def key_grad(i, _):
@@ -275,7 +280,7 @@
             dks[h, i] = nt(qmt[h, 0:HD, :], ds16[h, i]).astype(BF16)
         return 0
 
-    lax.fori_loop(0, RING, key_grad, 0)
+    lax.fori_loop(0, RING, key_grad, 0, unroll=4)
     for h in range(2):
         scatter(dks, dkr, h, 1 - h, 13)
 
@@ -377,6 +382,7 @@
         jax.ShapeDtypeStruct((TOK, COLS), BF16),
         jax.ShapeDtypeStruct((32, COLS), F32),
     )
+    operands = (queries, keys, values, cotangent, log_sum, chosen.transpose(2, 0, 1), normed_input)
     inside = pl.pallas_call(
         kernel,
         out_shape=shapes,
@@ -384,9 +390,9 @@
         out_specs=[pl.BlockSpec(memory_space=pltpu.VMEM)] * 4,
         scratch_shapes=scratch,
         compiler_params=pltpu.CompilerParams(
-            collective_id=0, has_side_effects=True, vmem_limit_bytes=55080 * 1024
+            collective_id=0, has_side_effects=True, vmem_limit_bytes=50 * 1024 * 1024
         ),
-    )(queries, keys, values, cotangent, log_sum, chosen.transpose(2, 0, 1), normed_input)
+    )(*[pltpu.with_memory_space_constraint(operand, pltpu.HBM) for operand in operands])
     return pl.pallas_call(
         write_out,
         out_shape=shapes,

time: 57.9 us -> 53.7 us (0.927)
  Pallas kernels: 55.3 us -> 52.9 us
  local copies, waits for them, and re-layouts: 1.41 us -> 0 us
    pallas_call x1, Pallas kernels: 54.6 us -> 52.2 us  [body(): pl.pallas_call(kernel, out_shape=shapes, in_specs=[pl.BlockSpec(memory_sp...]
    unnamed x4 -> x0, local copies, waits for them, and re-layouts: 1.41 us -> none
where the time goes in v4:
time: 53.7 us; the launch traced here: 53.5 us
  Pallas kernels  52.9 us (99%)
  between operations  0.64 us (1%)
    pallas_call x1, Pallas kernels, body(): pl.pallas_call(kernel, out_shape=shapes, in_specs=[pl.BlockSpec(memory_sp...  52.2 us

profile of v4, /device:TPU:6, one launch (start us, length us, event | category | flops | bytes accessed | tf_op | source)
XLA Modules:
  0.0 53.5 jit_solution(5033745370160677588)
XLA Ops:
  0.6 52.2 %shard_map.102 = (bf16[128,128]{1,0:T(8,128)(2,1)S(1)}, bf16[128,128]{1,0:T(8,128)(2,1)S(1)}, bf16[128,128]{1,0:T(8,128)(2,1)S(1)}, f32[32,128]{1,0:T(8,128)S(1)}) custom-call(bf16[128,128]{1,0:T(8,128)(2,1)} %q_in.1, bf16[128,128]{1,0:T(8,128)(2,1)} %k_in.1, bf16[128,128]{1,0:T(8,128)(2,1)} %v_in.1, bf16[128,128]{1,0:T(8,128)(2,1)} %g_in.1, ...), custom_call_target="tpu_custom_call" | custom-call | tf_op jit(solution)/shard_map/pallas_call | solution.py:386
  52.9 0.7 %shard_map.103 = (bf16[128,128]{1,0:T(8,128)(2,1)}, bf16[128,128]{1,0:T(8,128)(2,1)}, bf16[128,128]{1,0:T(8,128)(2,1)}, f32[32,128]{1,0:T(8,128)}) custom-call(bf16[128,128]{1,0:T(8,128)(2,1)S(1)} %get-tuple-element.8.a, bf16[128,128]{1,0:T(8,128)(2,1)S(1)} %get-tuple-element.9.b, bf16[128,128]{1,0:T(8,128)(2,1)S(1)} %get-tuple-element.10.c, ...), custom_call_target="tpu_custom_call" | custom-call | tf_op jit(solution)/shard_map/pallas_call | solution.py:396

commit v5 on v4

--- a/solution.py
+++ b/solution.py
@@ -58,9 +58,10 @@
         return POS[off % RING]
 
     barrier = pltpu.get_barrier_semaphore()
-    for off in range(1, RING):
-        for target in (along(0, off), along(1, off), (me, ring(tp, off))):
-            pl.semaphore_signal(barrier, inc=1, device_id=target, device_id_type=MESH)
+    greeted = [along(axis, off) for off in (1, -1, 2, -2) for axis in (0, 1)]
+    greeted += [(me, ring(tp, off)) for off in range(1, RING)]
+    for target in greeted:
+        pl.semaphore_signal(barrier, inc=1, device_id=target, device_id_type=MESH)
 
     loads = [
         pltpu.make_async_copy(src, dst, loc.at[n])
@@ -82,25 +83,23 @@
         buf[1, 0] = jnp.where(left, pltpu.roll(a, HD, 1), b).astype(BF16)
     for c in loads[4:]:
         c.wait()
-    pl.semaphore_wait(barrier, 3 * (RING - 1))
+    pl.semaphore_wait(barrier, len(greeted))
 
     def piece(axis, half):
-        return qg.at[axis] if half == 0 else kv.at[1 - axis]
-
-    steps = [(half, axis, d) for half in (0, 1) for axis in (0, 1) for d in (1, -1)]
+        return (qg.at[axis], kv.at[1 - axis], ls.at[axis])[half]
+
+    steps = [(half, axis, d) for half in (2, 0, 1) for axis in (0, 1) for d in (1, -1)]
 
     def group(off, half):
         near = (off + 4) % RING - 4
-        if abs(near) == 2:
-            return (0 if near < 0 else 2) + half
-        return {1: 4, 3: 6, 4: 8}[abs(near)] + half
+        return 3 * ((0 if near < 0 else 1) if abs(near) == 2 else {1: 2, 3: 3, 4: 4}[abs(near)]) + half
 
     def pass_on(axis, src, half, hop):
         buf = piece(axis, half)
         remote(
             buf.at[slot(src)],
             buf.at[slot(src - hop)],
-            done.at[2 * axis + half],
+            done.at[3 * axis + half],
             gather.at[axis, group(src - hop, half)],
             along(axis, hop),
         ).start()
@@ -109,11 +108,6 @@
         pass_on(axis, 0, half, 2 * d)
     for half, axis, d in steps:
         pass_on(axis, 0, half, d)
-    for off in FAR:
-        for axis in (0, 1):
-            remote(
-                ls.at[axis, 0], ls.at[axis, slot(-off)], done.at[4 + axis], come.at[4 + axis], along(axis, off)
-            ).start()
     for off in range(1, RING):
         remote(xg.at[0], xg.at[RING - off], done.at[6], come.at[6], (me, ring(tp, off))).start()
 
@@ -185,32 +179,29 @@
     strip(0, 0, 1, True)
 
     def arrive(axis, n, ref):
-        remote(ref, ref, done.at[2 * axis], gather.at[axis, n], along(axis, 1)).wait_recv()
+        remote(ref, ref, done.at[3 * axis], gather.at[axis, n], along(axis, 1)).wait_recv()
 
     rest = pl.ds(1, 7)
     for half, axis, d in steps:
         arrive(axis, group(-2 * d, half), piece(axis, half).at[slot(-2 * d)])
-        if half == (d < 0):
+        if half % 2 == (d < 0):
             pass_on(axis, -2 * d, half, 2 * d)
         pass_on(axis, -2 * d, half, d)
-    for axis in (0, 1):
-        part = ls.at[axis, rest]
-        remote(part, part, done.at[4 + axis], come.at[4 + axis], along(axis, 1)).wait_recv()
     stage(1)
     stage(2)
     strips(1, 3, 0, 3)
     strip(0, 1, 3)
-    for n, first in ((4, 3), (6, 5)):
+    for n, first in ((6, 3), (9, 5)):
         for axis in (0, 1):
-            for half in (0, 1):
+            for half in (0, 1, 2):
                 arrive(axis, n + half, piece(axis, half).at[pl.ds(first, 2)])
         stage(first)
         stage(first + 1)
         strips(first, first + 2, 0, first + 2)
         strips(0, first, first, first + 2)
     for axis in (0, 1):
-        for half in (0, 1):
-            arrive(axis, 8 + half, piece(axis, half).at[7])
+        for half in (0, 1, 2):
+            arrive(axis, 12 + half, piece(axis, half).at[7])
     stage(7)
     strip(7, 0, 8)
     strips(0, 7, 7, 8, unroll=7)
@@ -330,7 +321,7 @@
     gw_out[0:16, :] = summed(ha_s[y], ha_r, 17)
     gw_out[16:32, :] = summed(hb_s[z], hb_r, 18)
 
-    sent = [qg.at[0, rest], kv.at[1, rest], qg.at[1, rest], kv.at[0, rest], ls.at[0, rest], ls.at[1, rest]]
+    sent = [qg.at[0, rest], kv.at[1, rest], ls.at[0, rest], qg.at[1, rest], kv.at[0, rest], ls.at[1, rest]]
     sent += [xg.at[rest], dl.at[0, rest], dl.at[1, rest]]
     sent += [buf.at[h, rest] for buf in (dvs, dqs, dks) for h in range(2)]
     sent += [buf.at[rest] for buf in (gas, gbs, ha_s, hb_s)]
@@ -375,7 +366,7 @@
     scratch += [vm((2, 8, 64, 128), BF16)] * 6
     scratch += [vm((8, 8, 16, 128), BF16)] * 4
     scratch += [vm((8, 16, 128), BF16)] * 4
-    scratch += [dma((8,)), dma((2, 10)), dma((19,)), dma((19,))]
+    scratch += [dma((8,)), dma((2, 15)), dma((19,)), dma((19,))]
     shapes = (
         jax.ShapeDtypeStruct((TOK, COLS), BF16),
         jax.ShapeDtypeStruct((TOK, COLS), BF16),

time: 53.7 us -> 51.7 us (0.963)
  Pallas kernels: 52.9 us -> 50.5 us
    pallas_call x1, Pallas kernels: 52.2 us -> 49.9 us  [body(): pl.pallas_call(kernel, out_shape=shapes, in_specs=[pl.BlockSpec(memory_sp...]
where the time goes in v5:
time: 51.7 us; the launch traced here: 51.2 us
  Pallas kernels  50.5 us (98%)
  between operations  0.64 us (1%)
    pallas_call x1, Pallas kernels, body(): pl.pallas_call(kernel, out_shape=shapes, in_specs=[pl.BlockSpec(memory_sp...  49.9 us

profile of v5, /device:TPU:6, one launch (start us, length us, event | category | flops | bytes accessed | tf_op | source)
XLA Modules:
  0.0 51.2 jit_solution(1648109592313420583)
XLA Ops:
  0.6 49.9 %shard_map.102 = (bf16[128,128]{1,0:T(8,128)(2,1)S(1)}, bf16[128,128]{1,0:T(8,128)(2,1)S(1)}, bf16[128,128]{1,0:T(8,128)(2,1)S(1)}, f32[32,128]{1,0:T(8,128)S(1)}) custom-call(bf16[128,128]{1,0:T(8,128)(2,1)} %q_in.1, bf16[128,128]{1,0:T(8,128)(2,1)} %k_in.1, bf16[128,128]{1,0:T(8,128)(2,1)} %v_in.1, bf16[128,128]{1,0:T(8,128)(2,1)} %g_in.1, ...), custom_call_target="tpu_custom_call" | custom-call | tf_op jit(solution)/shard_map/pallas_call | solution.py:377
  50.5 0.7 %shard_map.103 = (bf16[128,128]{1,0:T(8,128)(2,1)}, bf16[128,128]{1,0:T(8,128)(2,1)}, bf16[128,128]{1,0:T(8,128)(2,1)}, f32[32,128]{1,0:T(8,128)}) custom-call(bf16[128,128]{1,0:T(8,128)(2,1)S(1)} %get-tuple-element.8.a, bf16[128,128]{1,0:T(8,128)(2,1)S(1)} %get-tuple-element.9.b, bf16[128,128]{1,0:T(8,128)(2,1)S(1)} %get-tuple-element.10.c, ...), custom_call_target="tpu_custom_call" | custom-call | tf_op jit(solution)/shard_map/pallas_call | solution.py:387

commit v6 on v5

--- a/solution.py
+++ b/solution.py
@@ -81,8 +81,8 @@
         a, b = raw[n].astype(F32), raw[n + 1].astype(F32)
         buf[0, 0] = jnp.where(left, a, pltpu.roll(b, HD, 1)).astype(BF16)
         buf[1, 0] = jnp.where(left, pltpu.roll(a, HD, 1), b).astype(BF16)
-    for c in loads[4:]:
-        c.wait()
+    loads[4].wait()
+    loads[5].wait()
     pl.semaphore_wait(barrier, len(greeted))
 
     def piece(axis, half):
@@ -108,6 +108,8 @@
         pass_on(axis, 0, half, 2 * d)
     for half, axis, d in steps:
         pass_on(axis, 0, half, d)
+    loads[6].wait()
+    loads[7].wait()
     for off in range(1, RING):
         remote(xg.at[0], xg.at[RING - off], done.at[6], come.at[6], (me, ring(tp, off))).start()
 
@@ -168,7 +170,7 @@
                     w16[h, i, :, into] = w.astype(BF16)
                     da[h, j] += jnp.sum((w * d).reshape(16, 8, TOK), axis=0)
 
-    def strips(first, last, lo, hi, unroll=1):
+    def strips(first, last, lo, hi, unroll=2):
         def one(i, _):
             strip(i, lo, hi)
             return 0
@@ -302,7 +304,6 @@
         remote(gbs.at[ring(y, off)], gbr.at[slot(-off)], done.at[16], come.at[16], along(0, off)).start()
 
     dv_out[...] = both_heads(dvs, dvr, 9).astype(BF16)
-    dk_out[...] = (both_heads(dks, dkr, 13) * 0.125).astype(BF16)
 
     def summed(own, arrived, n):
         part = arrived.at[rest]
@@ -318,6 +319,7 @@
     hb_s[...] = summed(gbs[y], gbr, 16).astype(BF16)
     for off in FAR:
         remote(hb_s.at[ring(z, off)], hb_r.at[slot(-off)], done.at[18], come.at[18], along(1, off)).start()
+    dk_out[...] = (both_heads(dks, dkr, 13) * 0.125).astype(BF16)
     gw_out[0:16, :] = summed(ha_s[y], ha_r, 17)
     gw_out[16:32, :] = summed(hb_s[z], hb_r, 18)
 

time: 51.7 us -> 51.1 us (0.988)
  Pallas kernels: 50.5 us -> 49.6 us
    pallas_call x1, Pallas kernels: 49.9 us -> 49 us  [body(): pl.pallas_call(kernel, out_shape=shapes, in_specs=[pl.BlockSpec(memory_sp...]
where the time goes in v6:
time: 51.1 us; the launch traced here: 50.3 us
  Pallas kernels  49.6 us (97%)
  between operations  0.64 us (1%)
    pallas_call x1, Pallas kernels, body(): pl.pallas_call(kernel, out_shape=shapes, in_specs=[pl.BlockSpec(memory_sp...  49 us

profile of v6, /device:TPU:6, one launch (start us, length us, event | category | flops | bytes accessed | tf_op | source)
XLA Modules:
  0.0 50.3 jit_solution(4767620788654394963)
XLA Ops:
  0.6 49.0 %shard_map.102 = (bf16[128,128]{1,0:T(8,128)(2,1)S(1)}, bf16[128,128]{1,0:T(8,128)(2,1)S(1)}, bf16[128,128]{1,0:T(8,128)(2,1)S(1)}, f32[32,128]{1,0:T(8,128)S(1)}) custom-call(bf16[128,128]{1,0:T(8,128)(2,1)} %q_in.1, bf16[128,128]{1,0:T(8,128)(2,1)} %k_in.1, bf16[128,128]{1,0:T(8,128)(2,1)} %v_in.1, bf16[128,128]{1,0:T(8,128)(2,1)} %g_in.1, ...), custom_call_target="tpu_custom_call" | custom-call | tf_op jit(solution)/shard_map/pallas_call | solution.py:379
  49.6 0.7 %shard_map.103 = (bf16[128,128]{1,0:T(8,128)(2,1)}, bf16[128,128]{1,0:T(8,128)(2,1)}, bf16[128,128]{1,0:T(8,128)(2,1)}, f32[32,128]{1,0:T(8,128)}) custom-call(bf16[128,128]{1,0:T(8,128)(2,1)S(1)} %get-tuple-element.8.a, bf16[128,128]{1,0:T(8,128)(2,1)S(1)} %get-tuple-element.9.b, bf16[128,128]{1,0:T(8,128)(2,1)S(1)} %get-tuple-element.10.c, ...), custom_call_target="tpu_custom_call" | custom-call | tf_op jit(solution)/shard_map/pallas_call | solution.py:389
